TPU v7x, 512 devices: a whole 4x4x16 slice. The times are simulated.
512 devices in a mesh: fs: 16 (over y, x), tp: 32 (over z, core).
Axes of the slice: x: 4, y: 4, z: 16, core: 2. Of those that a mesh axis runs over, the one named last changes fastest.
Arguments:
- saved_input: bfloat16 [16384, 4096], P('fs', 'tp'), may hold values from -6 to 6
- query_cot: bfloat16 [16384, 4096], P('fs', 'tp'), may hold values from -6 to 6
- key_cot: bfloat16 [16384, 4096], P('fs', 'tp'), may hold values from -6 to 6
- query_master: float32 [4096, 4096], P('fs', 'tp'), may hold values from -0.09375 to 0.09375
- key_master: float32 [4096, 4096], P('fs', 'tp'), may hold values from -0.09375 to 0.09375
- query_basis: bfloat16 [4096, 256], P('fs'), may hold values from -3 to 3
- key_basis: bfloat16 [4096, 256], P('fs'), may hold values from -3 to 3
- query_first: float32 [256, 4096], P('fs', 'tp'), may hold values from -240 to 240
- query_second: float32 [256, 4096], P('fs', 'tp'), may hold values from 1000 to 20000
- key_first: float32 [256, 4096], P('fs', 'tp'), may hold values from -240 to 240
- key_second: float32 [256, 4096], P('fs', 'tp'), may hold values from 1000 to 20000
Outputs:
- query_step: float32 [4096, 4096], P('fs', 'tp')
- query_weight: float32 [4096, 4096], P('fs', 'tp')
- query_copy: bfloat16 [4096, 4096], P(None, 'tp')
- query_first_new: float32 [256, 4096], P('fs', 'tp')
- query_second_new: float32 [256, 4096], P('fs', 'tp')
- key_step: float32 [4096, 4096], P('fs', 'tp')
- key_weight: float32 [4096, 4096], P('fs', 'tp')
- key_copy: bfloat16 [4096, 4096], P(None, 'tp')
- key_first_new: float32 [256, 4096], P('fs', 'tp')
- key_second_new: float32 [256, 4096], P('fs', 'tp')
All inputs are finite; a program needn't handle non-finite values.
Results may differ from a plain program's by a relative error of at most 0.0065.
Values may be sent and summed in bfloat16 or wider, within the bound.
A program may use at most 64 MiB of HBM per device.

v0:
```python
import jax
import jax.numpy as jnp
from jax import lax
from jax.sharding import Mesh
from jax.sharding import PartitionSpec as P

D = 4096
HD = 128
FS = ("fs_0", "fs_1")


moment_decay = 0.8
square_decay = 0.9
square_floor = 1.0
norm_floor = 0.01
step_rate = 0.01


def in_one_piece(arrays, axis, dim, along):
    widths = [a.shape[along] for a in arrays]
    both = jnp.concatenate(arrays, axis=along)
    out = lax.all_gather(both, axis, axis=dim, tiled=True)
    return tuple(jnp.split(out, [sum(widths[:k]) for k in range(1, len(widths))], axis=along))


def cut_along(x, dim, count):
    lengths = x.shape
    pieces = x.reshape(*lengths[:dim], count, lengths[dim] // count, *lengths[dim + 1 :])
    return jnp.moveaxis(pieces, dim, 0)


def sent_and_summed(x, axis, dim):
    count = lax.axis_size(axis)
    pieces = lax.all_to_all(cut_along(x, dim, count), axis, 0, 0, tiled=True)
    return jnp.sum(pieces, axis=0)


def sent_to_all(x, axis):
    count = lax.axis_size(axis)
    return lax.all_to_all(jnp.broadcast_to(x[None], (count, *x.shape)), axis, 0, 0, tiled=True)


def in_order(pieces, dim):
    lengths = list(pieces.shape[1:])
    lengths[dim] *= pieces.shape[0]
    return jnp.moveaxis(pieces, 0, dim).reshape(lengths)


def gathered_copies(x, axis, dim):
    pieces = sent_to_all(x, axis)
    return in_order(pieces, dim)


def by_axis(x, axes):
    for axis in axes:
        x = lax.psum(x, axis)
    return x


def split_product(low_part, cot_part):
    upper = low_part.astype(jnp.bfloat16)
    lower = (low_part - upper.astype(jnp.float32)).astype(jnp.bfloat16)
    return jnp.dot(upper.T, cot_part, preferred_element_type=jnp.float32) + jnp.dot(
        lower.T, cot_part, preferred_element_type=jnp.float32
    )


def cot_rows(query_low, key_low, cot_wide, width):

    def low_rows(start, count):
        return jnp.concatenate(
            [
                split_product(query_low, cot_wide[:, :width]),
                split_product(key_low, cot_wide[:, width:]),
            ],
            axis=1,
        )

    return low_rows


def head_squares(update):
    by_head = update.reshape(update.shape[0], -1, HD)
    return jnp.sum(by_head * by_head, axis=(0, 2))


def apply_scale(update, total):
    scale = 1.0 / jnp.sqrt(total / (D * HD) + norm_floor)
    by_head = update.reshape(update.shape[0], -1, HD)
    return (by_head * scale[None, :, None]).reshape(update.shape)


def body(
    saved_input,
    query_cot,
    key_cot,
    query_master,
    key_master,
    query_basis,
    key_basis,
    query_first,
    query_second,
    key_first,
    key_second,
):
    width = query_cot.shape[1]
    low_count = query_first.shape[0]
    cotangents = jnp.concatenate([query_cot, key_cot], axis=1)
    inputs = lax.all_gather(saved_input, "tp", axis=1, tiled=True)
    bases = in_one_piece((query_basis, key_basis), FS, 0, 1)
    query_low = jnp.dot(inputs, bases[0], preferred_element_type=jnp.float32)
    key_low = jnp.dot(inputs, bases[1], preferred_element_type=jnp.float32)
    low_rows = cot_rows(query_low, key_low, cotangents, width)
    projected = sent_and_summed(low_rows(jnp.int32(0), low_count * lax.axis_size(FS)), FS, 0)
    firsts = jnp.concatenate([query_first, key_first], axis=1)
    seconds = jnp.concatenate([query_second, key_second], axis=1)
    first_new = moment_decay * firsts + (1.0 - moment_decay) * projected
    second_new = square_decay * seconds + (1.0 - square_decay) * projected * projected
    ratio = (first_new / jnp.sqrt(second_new + square_floor)).astype(jnp.bfloat16)
    piece = gathered_copies(ratio, FS, 0)
    query_update = jnp.dot(query_basis, piece[:, :width], preferred_element_type=jnp.float32)
    key_update = jnp.dot(key_basis, piece[:, width:], preferred_element_type=jnp.float32)
    query_total, key_total = (
        by_axis(head_squares(query_update), FS),
        by_axis(head_squares(key_update), FS),
    )
    query_step = apply_scale(query_update, query_total)
    key_step = apply_scale(key_update, key_total)
    query_weight = query_master - step_rate * query_step
    key_weight = key_master - step_rate * key_step
    copies = in_one_piece(
        (query_weight.astype(jnp.bfloat16), key_weight.astype(jnp.bfloat16)), FS, 0, 1
    )
    return (
        query_step,
        query_weight,
        copies[0],
        first_new[:, :width],
        second_new[:, :width],
        key_step,
        key_weight,
        copies[1],
        first_new[:, width:],
        second_new[:, width:],
    )


def solution(mesh):
    torus = Mesh(mesh.devices.reshape(4, 4, mesh.shape["tp"]), ("fs_0", "fs_1", "tp"))
    in_specs = (
        P(FS, "tp"),
        P(FS, "tp"),
        P(FS, "tp"),
        P(FS, "tp"),
        P(FS, "tp"),
        P(FS, None),
        P(FS, None),
        P(FS, "tp"),
        P(FS, "tp"),
        P(FS, "tp"),
        P(FS, "tp"),
    )
    out_specs = (
        P(FS, "tp"),
        P(FS, "tp"),
        P(None, "tp"),
        P(FS, "tp"),
        P(FS, "tp"),
        P(FS, "tp"),
        P(FS, "tp"),
        P(None, "tp"),
        P(FS, "tp"),
        P(FS, "tp"),
    )
    return jax.shard_map(body, mesh=torus, in_specs=in_specs, out_specs=out_specs, check_vma=False)
```

profile of v0, /device:TPU:1, one launch (start us, length us, event | category | flops | bytes accessed | tf_op | source)
XLA Modules:
  0.0 306.6 jit_solution(4869370095504522026)
XLA Ops:
  7.2 1.7 pad_maximum_fusion
  9.0 0.7 all-gather.6.cloned.1.call-update
  9.7 73.7 %all-gather.4.cloned.1.call-done = bf16[4096,512]{1,0:T(8,128)(2,1)} async-done(((bf16[256,512]{1,0:T(8,128)(2,1)}), bf16[4096,512]{1,0:T(8,128)(2,1)}) %all-gather.4.cloned.1.call-update) | async-done | bytes 4194320 | tf_op jit(solution)/shard_map/all_gather | solution.py:22
  83.5 98.0 %all-gather.6.cloned.1.call-done = bf16[1024,4096]{1,0:T(8,128)(2,1)} async-done(((bf16[1024,128]{1,0:T(8,128)(2,1)}), bf16[1024,4096]{1,0:T(8,128)(2,1)}) %all-gather.6.cloned.1.call-update) | async-done | bytes 8388624 | tf_op jit(solution)/shard_map/all_gather | solution.py:109
  181.5 6.5 %fusion.4 = f32[1024,256]{0,1:T(8,128)S(1)} fusion(bf16[1024,4096]{1,0:T(8,128)(2,1)} %all-gather.6.cloned.1.call-done, bf16[4096,512]{1,0:T(8,128)(2,1)} %all-gather.4.cloned.1.call-done), kind=kOutput, calls=%fused_computation.4 | convolution fusion | flops 2147483648 | bytes 11534336 | tf_op jit(solution)/shard_map/dot_general | solution.py:111
  188.1 0.3 fusion.14
  188.4 0.3 convolution_add_fusion.1
  188.7 0.4 copy-done.11
  189.1 2.4 fusion.7
  191.6 0.3 fusion.11
  191.9 0.3 convolution_add_fusion
  192.3 0.1 copy.29
  192.4 14.6 %all_to_all.10 = f32[16,16,256]{2,1,0:T(8,128)S(1)} all-to-all(f32[16,16,256]{2,1,0:T(8,128)S(1)} %bitcast.24), channel_id=1, replica_groups=mesh['fs_0'=4,'fs_1'=4,'tp'=32] {'fs_0','fs_1'}, dimensions={0} | all-to-all | bytes 524288 | tf_op jit(solution)/shard_map/all_to_all | solution.py:34
  207.0 0.7 broadcast_in_dim.2
  207.7 3.5 %all-to-all-start.1 = ((bf16[16,16,256]{2,1,0:T(8,128)(2,1)}), bf16[16,16,256]{2,1,0:T(8,128)(2,1)S(1)}, u32[]{:S(2)}, u32[]{:S(2)}) async-start(bf16[16,16,256]{2,1,0:T(8,128)(2,1)} %broadcast_in_dim.2), calls=%async_computation.1 | async-start | bytes 262144 | tf_op jit(solution)/shard_map/all_to_all | solution.py:40
  211.3 0.1 copy.30
  211.4 0.1 copy.31
  211.5 6.6 %all-to-all-done.1 = bf16[16,16,256]{2,1,0:T(8,128)(2,1)S(1)} async-done(((bf16[16,16,256]{2,1,0:T(8,128)(2,1)}), bf16[16,16,256]{2,1,0:T(8,128)(2,1)S(1)}, u32[]{:S(2)}, u32[]{:S(2)}) %all-to-all-start.1) | async-done | bytes 131104 | tf_op jit(solution)/shard_map/all_to_all | solution.py:40
  218.1 0.8 multiply_reduce_fusion.1
  218.9 0.8 multiply_reduce_fusion
  219.7 7.1 %all-reduce.1 = (f32[1]{0:T(128)}, f32[1]{0:T(128)}) all-reduce(f32[1]{0:T(128)} %bitcast.4, f32[1]{0:T(128)} %bitcast.7), channel_id=1, replica_groups=mesh['fs_0'=4,'fs_1'=4,'tp'=32] {'fs_0'}, use_global_device_ids=true, to_apply=%region_2.0 | all-reduce | flops 2 | bytes 16 | tf_op jit(solution)/shard_map/psum | solution.py:56
  226.9 7.5 %all-reduce = (f32[1]{0:T(128)}, f32[1]{0:T(128)}) all-reduce(f32[1]{0:T(128)} %get-tuple-element.32, f32[1]{0:T(128)} %get-tuple-element.33), channel_id=1, replica_groups=mesh['fs_0'=4,'fs_1'=4,'tp'=32] {'fs_1'}, use_global_device_ids=true, to_apply=%region_3.0 | all-reduce | flops 2 | bytes 16 | tf_op jit(solution)/shard_map/psum | solution.py:56
  235.8 0.7 pad_maximum_fusion.2
  236.5 0.6 fusion.27
  237.1 0.8 copy.32
  237.9 0.8 copy.33
  238.6 0.8 copy.35
  239.4 0.8 copy.36
  240.2 55.6 %all-gather.8.cloned.1.call-done = bf16[4096,256]{0,1:T(8,128)(2,1)} async-done(((bf16[256,256]{0,1:T(8,128)(2,1)}), bf16[4096,256]{0,1:T(8,128)(2,1)}) %all-gather.8.cloned.1.call-update) | async-done | bytes 2097168 | tf_op jit(solution)/shard_map/all_gather | solution.py:22
  295.8 1.7 fusion.26
  297.4 1.3 copy.34
  298.7 1.3 copy.37
  (32 shorter events, 0.3 us)
Async XLA Ops:
  7.2 180.9 %copy-start = (bf16[1024,128]{1,0:T(8,128)(2,1)S(1)}, bf16[1024,128]{1,0:T(8,128)(2,1)}, u32[]{:S(2)}) copy-start(bf16[1024,128]{1,0:T(8,128)(2,1)} %param.12) | copy-start | bytes 786436
  7.2 76.3 %all-gather.4.cloned.1.call-start = ((), (), s32[]{:S(2)}) async-start(), calls=%async_computation.2 | async-start | bytes 4456448 | tf_op jit(solution)/shard_map/all_gather | solution.py:22
  9.0 172.5 %all-gather.6.cloned.1.call-start = ((), (), s32[]{:S(2)}) async-start(), calls=%async_computation.3 | async-start | bytes 8650752 | tf_op jit(solution)/shard_map/all_gather | solution.py:109
  181.5 7.2 %copy-start.10 = (bf16[1024,4096]{1,0:T(8,128)(2,1)S(1)}, bf16[1024,4096]{1,0:T(8,128)(2,1)}, u32[]{:S(2)}) copy-start(bf16[1024,4096]{1,0:T(8,128)(2,1)} %all-gather.6.cloned.1.call-done) | copy-start | bytes 25165828
  181.5 7.6 %copy-start.11 = (bf16[4096,512]{1,0:T(8,128)(2,1)S(1)}, bf16[4096,512]{1,0:T(8,128)(2,1)}, u32[]{:S(2)}) copy-start(bf16[4096,512]{1,0:T(8,128)(2,1)} %all-gather.4.cloned.1.call-done) | copy-start | bytes 12582916
  189.1 2.4 copy-start.1
  191.5 15.5 %copy-start.6 = (f32[16,128]{1,0:T(8,128)S(1)}, f32[16,128]{1,0:T(8,128)}, u32[]{:S(2)}) copy-start(f32[16,128]{1,0:T(8,128)} %param.21) | copy-start | bytes 24580
  191.5 15.5 %copy-start.7 = (f32[16,128]{1,0:T(8,128)S(1)}, f32[16,128]{1,0:T(8,128)}, u32[]{:S(2)}) copy-start(f32[16,128]{1,0:T(8,128)} %param.19) | copy-start | bytes 24580
  191.5 15.5 %copy-start.8 = (f32[16,128]{1,0:T(8,128)S(1)}, f32[16,128]{1,0:T(8,128)}, u32[]{:S(2)}) copy-start(f32[16,128]{1,0:T(8,128)} %param.20) | copy-start | bytes 24580
  191.5 15.5 %copy-start.9 = (f32[16,128]{1,0:T(8,128)S(1)}, f32[16,128]{1,0:T(8,128)}, u32[]{:S(2)}) copy-start(f32[16,128]{1,0:T(8,128)} %param.18) | copy-start | bytes 24580
  191.5 19.7 %copy-start.4 = (f32[256,128]{1,0:T(8,128)S(1)}, f32[256,128]{1,0:T(8,128)}, u32[]{:S(2)}) copy-start(f32[256,128]{1,0:T(8,128)} %param.14) | copy-start | bytes 393220
  191.5 19.8 %copy-start.5 = (f32[256,128]{1,0:T(8,128)S(1)}, f32[256,128]{1,0:T(8,128)}, u32[]{:S(2)}) copy-start(f32[256,128]{1,0:T(8,128)} %param.15) | copy-start | bytes 393220
  191.6 26.5 %copy-start.2 = (bf16[256,256]{1,0:T(8,128)(2,1)S(1)}, bf16[256,256]{1,0:T(8,128)(2,1)}, u32[]{:S(2)}) copy-start(bf16[256,256]{1,0:T(8,128)(2,1)} %param.16) | copy-start | bytes 393220
  191.6 27.4 %copy-start.3 = (bf16[256,256]{1,0:T(8,128)(2,1)S(1)}, bf16[256,256]{1,0:T(8,128)(2,1)}, u32[]{:S(2)}) copy-start(bf16[256,256]{1,0:T(8,128)(2,1)} %param.17) | copy-start | bytes 393220
  207.7 10.4 %all-to-all-start.1 = ((bf16[16,16,256]{2,1,0:T(8,128)(2,1)}), bf16[16,16,256]{2,1,0:T(8,128)(2,1)S(1)}, u32[]{:S(2)}, u32[]{:S(2)}) async-start(bf16[16,16,256]{2,1,0:T(8,128)(2,1)} %broadcast_in_dim.2), calls=%async_computation.1 | async-start | bytes 262144 | tf_op jit(solution)/shard_map/all_to_all | solution.py:40
  211.2 84.5 %all-gather.8.cloned.1.call-start = ((), (), s32[]{:S(2)}) async-start(), calls=%async_computation.4 | async-start | bytes 2228224 | tf_op jit(solution)/shard_map/all_gather | solution.py:22
Sparse Core Ops, SparseCore 0:
  11.6 71.8 all-gather.3
  85.5 95.9 all-gather.5
  236.6 59.0 all-gather.7
where the time goes:
time: 307 us
  waiting for transfers between devices  235 us (77%)
  blocking collectives  29.2 us (10%)
  between operations  15.4 us (5%)
  matrix products  11.8 us (4%)
  local copies, waits for them, and re-layouts  9.34 us (3%)
  starting transfers between devices  3.63 us (1%)
    all_gather x2, waiting for transfers between devices, in_one_piece(): out = lax.all_gather(both, axis, axis=dim, tiled=True)  129 us
    all_gather x1, waiting for transfers between devices, body(): inputs = lax.all_gather(saved_input, 'tp', axis=1, tiled=True)  98 us
    psum x2, blocking collectives, by_axis(): x = lax.psum(x, axis)  14.7 us
    all_to_all x1, blocking collectives, sent_and_summed(): pieces = lax.all_to_all(cut_along(x, dim, count), axis, 0, 0, tiled=True)  14.6 us
    all_to_all x1, waiting for transfers between devices, sent_to_all(): lax.all_to_all(jnp.broadcast_to(x[None], (count, *x.shape)), axis, 0, 0,...  6.6 us
    dot_general x1, matrix products, body(): query_low = jnp.dot(inputs, bases[0], preferred_element_type=jnp.float32)  6.54 us
    unnamed x32, local copies, waits for them, and re-layouts  6.25 us
  transfers between devices with their start and end apart: 4, of which 4 were waited for; matrix products, arithmetic and copies ran while one was open for 1% of the time, Pallas kernels for 0%

commit v1 on v0

v1 whole, which is shorter than its diff:
```python
import jax
import jax.numpy as jnp
from jax import lax
from jax.experimental import pallas as pl
from jax.experimental.pallas import tpu as pltpu
from jax.sharding import Mesh
from jax.sharding import PartitionSpec as P

D = 4096
HD = 128
RANK = 256
YN, XN, ZN, CN = 4, 4, 16, 2
FN = YN * XN
TOK = 1024
SUB = TOK // ZN
ROWS = D // FN
HALF = ROWS // CN
LOW = RANK // FN
AXES = ("y", "x", "z", "c")
FS = ("y", "x")
TP = ("z", "c")

moment_decay = 0.8
square_decay = 0.9
square_floor = 1.0
norm_floor = 0.01
step_rate = 0.01

MESH_ID = pl.DeviceIdType.MESH
BF = jnp.bfloat16
F32 = jnp.float32

PLANE = sorted(
    [(dy, dx) for dy in range(YN) for dx in range(XN) if (dy, dx) != (0, 0)],
    key=lambda o: -(min(o[0], 4 - o[0]) + min(o[1], 4 - o[1])),
)
ALONG_Z = [8, 7, -7, 6, -6, 5, -5, 4, -4, 3, -3, 2, -2, 1, -1]
Z_FIRST = [6, -6, 3, -3, 1, -1]
Z_RELAY = [(3, (1, -1)), (-3, (-1, 1)), (6, (2, 1, -1)), (-6, (-1, 1))]


class Sends:
    def __init__(self, send_sem, recv_sem):
        self.send_sem, self.recv_sem = send_sem, recv_sem
        self.count = 0
        self.started = []

    def take(self):
        self.count += 1
        return self.count - 1

    def start(self, number, src, dst, device):
        copy = pltpu.make_async_remote_copy(
            src_ref=src,
            dst_ref=dst,
            send_sem=self.send_sem.at[number],
            recv_sem=self.recv_sem.at[number],
            device_id=device,
            device_id_type=MESH_ID,
        )
        copy.start()
        self.started.append(copy)

    def landed(self, number, dst, device):
        pltpu.make_async_remote_copy(
            src_ref=dst,
            dst_ref=dst,
            send_sem=self.send_sem.at[number],
            recv_sem=self.recv_sem.at[number],
            device_id=device,
            device_id_type=MESH_ID,
        ).wait_recv()

    def finish(self):
        for copy in self.started:
            copy.wait_send()


def wrap(value, count):
    return lax.rem(value + 2 * count, count)


def plane_gather(sends, piece, me, rows):
    y, x, z, c = me
    half, quarter = rows // 2, rows // 4
    signs = (1, -1)

    def shift(h, first, second):
        d1, d2 = (first, second)
        dy, dx = (d2, d1) if h == 0 else (d1, d2)
        return wrap(y + dy, YN), wrap(x + dx, XN)

    def ref(h, first, second, part=None):
        fy, fx = shift(h, first, second)
        start = h * half + (0 if part is None else part * quarter)
        return piece(fy, fx, start, half if part is None else quarter)

    def dev(h, first, second):
        fy, fx = shift(h, first, second)
        return (fy, fx, z, c)

    part_of = {1: 0, -1: 1}
    both = [(h, s) for h in (0, 1) for s in signs]
    n1 = {k: sends.take() for k in both}
    n1r = {k: sends.take() for k in both}
    n2 = {(h, j, s): sends.take() for j in (0, -1, 1, 2) for h, s in both}
    n2r = {(h, j, s): sends.take() for j in (0, -1, 1, 2) for h, s in both}

    def second_stage(h, j):
        for s in signs:
            sends.start(n2[h, j, s], ref(h, j, 0), ref(h, j, 0), dev(h, 0, s))

    def second_relay(h, j):
        for s in signs:
            sends.landed(n2[h, j, s], ref(h, j, -s), dev(h, 0, s))
            p = part_of[s]
            sends.start(n2r[h, j, s], ref(h, j, -s, p), ref(h, j, -s, p), dev(h, 0, s))

    for h, s in both:
        sends.start(n1[h, s], ref(h, 0, 0), ref(h, 0, 0), dev(h, s, 0))
    for h in (0, 1):
        second_stage(h, 0)
    yield
    for h, s in both:
        sends.landed(n1[h, s], ref(h, -s, 0), dev(h, s, 0))
        p = part_of[s]
        sends.start(n1r[h, s], ref(h, -s, 0, p), ref(h, -s, 0, p), dev(h, s, 0))
        second_stage(h, -s)
    yield
    for h in (0, 1):
        second_relay(h, 0)
    yield
    for h in (0, 1):
        for s in signs:
            p = part_of[s]
            sends.landed(n1r[h, s], ref(h, 2, 0, p), dev(h, s, 0))
        second_stage(h, 2)
    yield
    for j in (-1, 1):
        for h in (0, 1):
            second_relay(h, j)
    yield
    for h in (0, 1):
        second_relay(h, 2)
    yield
    for j in (0, -1, 1, 2):
        for h, s in both:
            p = part_of[s]
            sends.landed(n2r[h, j, s], ref(h, j, 2, p), dev(h, s, 0))


def exchange(
    x_in, qc_in, kc_in, qm_in, km_in, qb_in, kb_in, qf_in, qs_in, kf_in, ks_in,
    basis, masters, ratios, moments_out,
    xs, xg, cots, cot_other, cot_rel, cot_t, mas, mom, mom_other,
    psend, precv, xb, lowp, lowr, rsend, msend,
    load_sem, send_sem, recv_sem,
):
    y, x, z, c = (lax.axis_index(a) for a in AXES)
    me = (y, x, z, c)
    oc = 1 - c
    f = y * XN + x
    partner = (y, x, z, oc)

    barrier = pltpu.get_barrier_semaphore()
    near = [(wrap(y + dy, YN), wrap(x + dx, XN), z, c) for dy, dx in PLANE]
    near += [(wrap(y + dy, YN), wrap(x + dx, XN), z, oc) for dy, dx in PLANE]
    near += [partner]
    near += [(y, x, wrap(z + d, ZN), c) for d in ALONG_Z]
    for device in near:
        pl.semaphore_signal(barrier, inc=1, device_id=device, device_id_type=MESH_ID)

    loads = []

    def load(src, dst):
        copy = pltpu.make_async_copy(src, dst, load_sem.at[len(loads)])
        copy.start()
        loads.append(copy)

    mine = pl.ds(pl.multiple_of(c * HALF, HALF), HALF)
    load(x_in, xs)
    load(qb_in.at[mine], basis.at[f, c, :, pl.ds(0, RANK)])
    load(kb_in.at[mine], basis.at[f, c, :, pl.ds(RANK, RANK)])
    load(qc_in, cots.at[0])
    load(kc_in, cots.at[1])
    load(qf_in, mom.at[0, 0])
    load(qs_in, mom.at[0, 1])
    load(kf_in, mom.at[1, 0])
    load(ks_in, mom.at[1, 1])
    load(qm_in, mas.at[0])
    load(km_in, mas.at[1])
    for copy in loads:
        copy.wait()
    masters[f, :, 0:HD] = mas[0].astype(BF)
    masters[f, :, HD : 2 * HD] = mas[1].astype(BF)

    sends = Sends(send_sem, recv_sem)
    pl.semaphore_wait(barrier, len(near))

    def xslot(zz):
        return xg.at[:, pl.ds(pl.multiple_of(zz * HD, HD), HD)]

    nx = {d: sends.take() for d in ALONG_Z}
    gather_basis = plane_gather(
        sends, lambda fy, fx, s, n: basis.at[fy * XN + fx, c, pl.ds(s, n)], me, HALF
    )
    gather_masters = plane_gather(
        sends, lambda fy, fx, s, n: masters.at[fy * XN + fx, pl.ds(s, n)], me, ROWS
    )
    next(gather_basis)
    for d in ALONG_Z:
        zz = wrap(z + d, ZN)
        rows = xs.at[pl.ds(pl.multiple_of(zz * SUB, SUB), SUB)]
        sends.start(nx[d], rows, xslot(z), (y, x, zz, c))
    n_cot, n_mom = sends.take(), sends.take()
    sends.start(n_cot, cots.at[oc], cot_other, partner)
    sends.start(n_mom, mom.at[oc], mom_other, partner)
    xg[:, pl.ds(pl.multiple_of(z * HD, HD), HD)] = xs[pl.ds(pl.multiple_of(z * SUB, SUB), SUB), :]
    next(gather_basis)

    sends.landed(n_cot, cot_other, partner)
    sends.landed(n_mom, mom_other, partner)
    for o in range(ZN):
        zz = wrap(z - o, ZN)
        rows = pl.ds(pl.multiple_of(zz * SUB, SUB), SUB)
        cot_rel[o * SUB : (o + 1) * SUB, 0:HD] = cots[c, rows, :]
        cot_rel[o * SUB : (o + 1) * SUB, HD : 2 * HD] = cot_other[rows, :]
    next(gather_basis)
    next(gather_basis)
    cot_t[...] = cot_rel[...].T
    for _ in gather_basis:
        pass
    next(gather_masters)
    for d in ALONG_Z:
        sends.landed(nx[d], xslot(wrap(z - d, ZN)), partner)

    part = jnp.zeros((SUB, 2 * RANK), F32)
    for k in range(FN // 2):
        rows = basis[2 * k : 2 * k + 2, c].reshape(2 * HALF, 2 * RANK)
        part += jnp.dot(
            xg[:, k * 2 * HD : (k + 1) * 2 * HD], rows, preferred_element_type=F32
        )
    psend[0] = part[:, :RANK]
    psend[1] = part[:, RANK:]
    n_part = sends.take()
    sends.start(n_part, psend.at[oc], precv, partner)
    n_basis = sends.take()
    sends.landed(n_part, precv, partner)
    xb[0] = (psend[c] + precv[...]).astype(BF)

    nz = {}
    for d in Z_FIRST:
        nz[d % ZN] = sends.take()
    for o, hops in Z_RELAY:
        for d in hops:
            nz[(o + d) % ZN] = sends.take()
    seen = set()

    def z_send(o, d):
        sends.start(
            nz[(o + d) % ZN], xb.at[o % ZN], xb.at[(o + d) % ZN], (y, x, wrap(z + d, ZN), c)
        )

    def z_landed(o):
        if o % ZN not in seen:
            seen.add(o % ZN)
            sends.landed(nz[o % ZN], xb.at[o % ZN], partner)

    for d in Z_FIRST:
        z_send(0, d)
    sends.start(n_basis, basis.at[:, c], basis.at[:, c], partner)
    next(gather_masters)
    for o, hops in Z_RELAY[:2]:
        z_landed(o)
        for d in hops:
            z_send(o, d)
    for o, hops in Z_RELAY[2:]:
        z_landed(o)
        for d in hops:
            z_send(o, d)
    next(gather_masters)
    next(gather_masters)
    next(gather_masters)
    for o in range(1, ZN):
        z_landed(o)

    low_t = jnp.dot(cot_t[...], xb[...].reshape(TOK, RANK), preferred_element_type=F32)
    lowp[...] = low_t.T.reshape(FN, LOW, 2 * HD)
    nl = {p: sends.take() for p in PLANE}
    for dy, dx in PLANE:
        ty, tx = wrap(y + dy, YN), wrap(x + dx, XN)
        sends.start(nl[dy, dx], lowp.at[ty * XN + tx], lowr.at[dy * XN + dx], (ty, tx, z, c))
    next(gather_masters)
    low = lowp[f]
    for dy, dx in PLANE:
        sends.landed(nl[dy, dx], lowr.at[dy * XN + dx], partner)
        low = low + lowr[dy * XN + dx]

    nr = {(p, k): sends.take() for p in [(0, 0)] + PLANE for k in (0, 1)}
    n_out = sends.take()
    for k, (first, second) in enumerate(
        ((mom[c, 0], mom[c, 1]), (mom_other[0], mom_other[1]))
    ):
        part = low[:, k * HD : (k + 1) * HD]
        first_new = moment_decay * first + (1.0 - moment_decay) * part
        second_new = square_decay * second + (1.0 - square_decay) * part * part
        rsend[k] = (first_new / jnp.sqrt(second_new + square_floor)).astype(BF)
        if k == 0:
            moments_out[c, 0] = first_new
            moments_out[c, 1] = second_new
        else:
            msend[0] = first_new
            msend[1] = second_new
    ratios[c, f] = rsend[0]
    for dy, dx in PLANE + [(0, 0)]:
        ty, tx = wrap(y + dy, YN), wrap(x + dx, XN)
        for k, core in ((0, c), (1, oc)):
            if k == 0 and (dy, dx) == (0, 0):
                continue
            sends.start(nr[(dy, dx), k], rsend.at[k], ratios.at[c, f], (ty, tx, z, core))
    sends.start(n_out, msend, moments_out.at[c], partner)
    for _ in gather_masters:
        pass
    sends.landed(n_basis, basis.at[:, oc], partner)
    for dy, dx in PLANE + [(0, 0)]:
        sy, sx = wrap(y - dy, YN), wrap(x - dx, XN)
        for k in (0, 1):
            if k == 0 and (dy, dx) == (0, 0):
                continue
            m = c if k == 0 else oc
            sends.landed(nr[(dy, dx), k], ratios.at[m, sy * XN + sx], partner)
    sends.landed(n_out, moments_out.at[oc], partner)
    sends.finish()


N_SENDS = 15 + 80 + 2 + 2 + 15 + 15 + 32 + 1


def finish(
    basis, masters, ratios, moments, qm, km,
    q_step, q_weight, q_copy, q_first, q_second,
    k_step, k_weight, k_copy, k_first, k_second,
    held,
):
    f = lax.axis_index("y") * XN + lax.axis_index("x")
    outs = (
        (qm, q_step, q_weight, q_copy, q_first, q_second),
        (km, k_step, k_weight, k_copy, k_first, k_second),
    )
    for m, (master, step_ref, weight_ref, copy_ref, first_ref, second_ref) in enumerate(outs):
        first_ref[...] = moments[m, 0]
        second_ref[...] = moments[m, 1]
        ratio = ratios[m].reshape(RANK, HD)

        def product(k, total):
            rows = basis[k, :, :, m * RANK : (m + 1) * RANK].reshape(ROWS, RANK)
            update = jnp.dot(rows, ratio, preferred_element_type=F32)
            held[k] = update
            return total + jnp.sum((update * update).reshape(ROWS // 8, 8, HD), axis=0)

        total = lax.fori_loop(0, FN, product, jnp.zeros((8, HD), F32), unroll=2)
        scale = 1.0 / jnp.sqrt(jnp.sum(total) / (D * HD) + norm_floor)

        def scaled(k, _):
            step = held[k] * scale
            old = masters[k, :, m * HD : (m + 1) * HD].astype(F32)
            copy_ref[pl.ds(pl.multiple_of(k * ROWS, ROWS), ROWS), :] = (
                old - step_rate * step
            ).astype(BF)
            return 0

        lax.fori_loop(0, FN, scaled, 0)
        step = held[f] * scale
        step_ref[...] = step
        weight_ref[...] = master[...] - step_rate * step


def body(*args):
    any_space = pl.BlockSpec(memory_space=pl.ANY)
    vmem = pl.BlockSpec(memory_space=pltpu.VMEM)
    dma = pltpu.SemaphoreType.DMA
    basis, masters, ratios, moments = pl.pallas_call(
        exchange,
        name="exchange",
        out_shape=(
            jax.ShapeDtypeStruct((FN, CN, HALF, 2 * RANK), BF),
            jax.ShapeDtypeStruct((FN, ROWS, 2 * HD), BF),
            jax.ShapeDtypeStruct((2, FN, LOW, HD), BF),
            jax.ShapeDtypeStruct((2, 2, LOW, HD), F32),
        ),
        in_specs=[any_space] * len(args),
        out_specs=(vmem,) * 4,
        scratch_shapes=[
            pltpu.VMEM((TOK, HD), BF),
            pltpu.VMEM((SUB, ZN * HD), BF),
            pltpu.VMEM((2, TOK, HD), BF),
            pltpu.VMEM((TOK, HD), BF),
            pltpu.VMEM((TOK, 2 * HD), BF),
            pltpu.VMEM((2 * HD, TOK), BF),
            pltpu.VMEM((2, ROWS, HD), F32),
            pltpu.VMEM((2, 2, LOW, HD), F32),
            pltpu.VMEM((2, LOW, HD), F32),
            pltpu.VMEM((2, SUB, RANK), F32),
            pltpu.VMEM((SUB, RANK), F32),
            pltpu.VMEM((ZN, SUB, RANK), BF),
            pltpu.VMEM((FN, LOW, 2 * HD), F32),
            pltpu.VMEM((FN, LOW, 2 * HD), F32),
            pltpu.VMEM((2, LOW, HD), BF),
            pltpu.VMEM((2, LOW, HD), F32),
            dma((11,)),
            dma((N_SENDS,)),
            dma((N_SENDS,)),
        ],
        compiler_params=pltpu.CompilerParams(
            collective_id=0, has_side_effects=True, vmem_limit_bytes=48 * 1024 * 1024
        ),
    )(*args)
    matrix = jax.ShapeDtypeStruct((ROWS, HD), F32)
    whole = jax.ShapeDtypeStruct((D, HD), BF)
    moment = jax.ShapeDtypeStruct((LOW, HD), F32)
    return pl.pallas_call(
        finish,
        name="finish",
        out_shape=(matrix, matrix, whole, moment, moment) * 2,
        in_specs=[vmem] * 6,
        out_specs=(vmem,) * 10,
        scratch_shapes=[pltpu.VMEM((FN, ROWS, HD), F32)],
        compiler_params=pltpu.CompilerParams(vmem_limit_bytes=48 * 1024 * 1024),
    )(basis, masters, ratios, moments, args[3], args[4])


def solution(mesh):
    torus = Mesh(mesh.devices.reshape(YN, XN, ZN, CN), AXES)
    split = P(FS, TP)
    in_specs = (split,) * 5 + (P(FS, None),) * 2 + (split,) * 4
    out_specs = (split, split, P(None, TP), split, split) * 2
    return jax.shard_map(body, mesh=torus, in_specs=in_specs, out_specs=out_specs, check_vma=False)
```

time: 307 us -> 85.1 us (0.28)
  waiting for transfers between devices: 235 us -> 0 us
  Pallas kernels: 0 us -> 74.7 us
  blocking collectives: 29.2 us -> 0 us
  between operations: 15.4 us -> 0.67 us
  matrix products: 11.8 us -> 0 us
  starting transfers between devices: 3.63 us -> 0 us
    all_gather x3 -> x0, waiting for transfers between devices: 227 us -> none  [the longest x2 129 us: in_one_piece(): out = lax.all_gather(both, axis, axis=dim, tiled=True)]
    pallas_call x0 -> x2, Pallas kernels: none -> 74.7 us  [the longest x1 66.3 us: body(): pl.pallas_call(exchange, name='exchange', out_shape=(jax.ShapeDtypeStruct...]
    psum x2 -> x0, blocking collectives: 14.7 us -> none  [by_axis(): x = lax.psum(x, axis)]
    all_to_all x1 -> x0, blocking collectives: 14.6 us -> none  [sent_and_summed(): pieces = lax.all_to_all(cut_along(x, dim, count), axis, 0, 0, tiled=True)]
    dot_general x8 -> x0, matrix products: 11.8 us -> none  [the longest x1 6.54 us: body(): query_low = jnp.dot(inputs, bases[0], preferred_element_type=jnp.float32)]
    all_to_all x1 -> x0, waiting for transfers between devices: 6.6 us -> none  [sent_to_all(): lax.all_to_all(jnp.broadcast_to(x[None], (count, *x.shape)), axis, 0, 0,...]
    all_to_all x1 -> x0, starting transfers between devices: 3.51 us -> none  [sent_to_all(): lax.all_to_all(jnp.broadcast_to(x[None], (count, *x.shape)), axis, 0, 0,...]
    unnamed x32 -> x22, local copies, waits for them, and re-layouts: 6.25 us -> 9.24 us
  transfers between devices with their start and end apart: 4 -> 0, of which waited for: 4 -> 0; matrix products, arithmetic and copies ran while one was open for 1% -> 0% of each run, Pallas kernels for 0% -> 0%
where the time goes in v1:
time: 85.1 us; the launch traced here: 84.6 us
  Pallas kernels  74.7 us (88%)
  local copies, waits for them, and re-layouts  9.24 us (11%)
    pallas_call x1, Pallas kernels, body(): pl.pallas_call(exchange, name='exchange', out_shape=(jax.ShapeDtypeStruct...  66.3 us
    unnamed x22, local copies, waits for them, and re-layouts  9.24 us
    pallas_call x1, Pallas kernels, body(): pl.pallas_call(finish, name='finish', out_shape=(matrix, matrix, whole, m...  8.35 us

profile of v1, /device:TPU:1, one launch (start us, length us, event | category | flops | bytes accessed | tf_op | source)
XLA Modules:
  0.0 84.6 jit_solution(2238401299146623678)
XLA Ops:
  0.6 0.0 copy-start
  0.7 0.9 %copy-done = f32[256,128]{1,0:T(8,128)S(1)} copy-done((f32[256,128]{1,0:T(8,128)S(1)}, f32[256,128]{1,0:T(8,128)}, u32[]{:S(2)}) %copy-start) | copy-done | bytes 131096
  1.6 0.0 copy-start.1
  1.6 0.9 %copy-done.1 = f32[256,128]{1,0:T(8,128)S(1)} copy-done((f32[256,128]{1,0:T(8,128)S(1)}, f32[256,128]{1,0:T(8,128)}, u32[]{:S(2)}) %copy-start.1) | copy-done | bytes 131096
  2.5 0.0 copy-start.2
  2.5 0.9 %copy-done.2 = bf16[1024,128]{1,0:T(8,128)(2,1)S(1)} copy-done((bf16[1024,128]{1,0:T(8,128)(2,1)S(1)}, bf16[1024,128]{1,0:T(8,128)(2,1)}, u32[]{:S(2)}) %copy-start.2) | copy-done | bytes 262168
  3.4 0.0 copy-start.3
  3.4 0.9 %copy-done.3 = bf16[1024,128]{1,0:T(8,128)(2,1)S(1)} copy-done((bf16[1024,128]{1,0:T(8,128)(2,1)S(1)}, bf16[1024,128]{1,0:T(8,128)(2,1)}, u32[]{:S(2)}) %copy-start.3) | copy-done | bytes 262168
  4.4 0.0 copy-start.4
  4.4 0.9 %copy-done.4 = bf16[1024,128]{1,0:T(8,128)(2,1)S(1)} copy-done((bf16[1024,128]{1,0:T(8,128)(2,1)S(1)}, bf16[1024,128]{1,0:T(8,128)(2,1)}, u32[]{:S(2)}) %copy-start.4) | copy-done | bytes 262168
  5.3 0.0 copy-start.5
  5.3 0.9 %copy-done.5 = bf16[256,256]{1,0:T(8,128)(2,1)S(1)} copy-done((bf16[256,256]{1,0:T(8,128)(2,1)S(1)}, bf16[256,256]{1,0:T(8,128)(2,1)}, u32[]{:S(2)}) %copy-start.5) | copy-done | bytes 131096
  6.2 0.0 copy-start.6
  6.2 0.9 %copy-done.6 = bf16[256,256]{1,0:T(8,128)(2,1)S(1)} copy-done((bf16[256,256]{1,0:T(8,128)(2,1)S(1)}, bf16[256,256]{1,0:T(8,128)(2,1)}, u32[]{:S(2)}) %copy-start.6) | copy-done | bytes 131096
  7.1 0.0 copy-start.7
  7.1 0.7 copy-done.7
  7.8 0.0 copy-start.8
  7.8 0.7 copy-done.8
  8.5 0.0 copy-start.9
  8.5 0.7 copy-done.9
  9.2 0.0 copy-start.10
  9.2 0.7 copy-done.10
  9.9 66.3 %exchange.1 = (bf16[16,2,128,512]{3,2,1,0:T(8,128)(2,1)}, bf16[16,256,256]{2,1,0:T(8,128)(2,1)S(1)}, bf16[2,16,16,128]{3,2,1,0:T(8,128)(2,1)S(1)}, f32[2,2,16,128]{3,2,1,0:T(8,128)S(1)}) custom-call(bf16[1024,128]{1,0:T(8,128)(2,1)S(1)} %copy-done.2, bf16[1024,128]{1,0:T(8,128)(2,1)S(1)} %copy-done.3, bf16[1024,128]{1,0:T(8,128)(2,1)S(1)} %copy-done.4, ...), custom_call_target="tpu_custom_call" | custom-call | tf_op jit(solution)/shard_map/exchange/pallas_call | solution.py:382
  76.2 8.3 %finish.1 = (f32[256,128]{1,0:T(8,128)}, f32[256,128]{1,0:T(8,128)}, bf16[4096,128]{1,0:T(8,128)(2,1)}, f32[16,128]{1,0:T(8,128)}, f32[16,128]{1,0:T(8,128)}, /*...) custom-call(bf16[16,2,128,512]{3,2,1,0:T(8,128)(2,1)} %get-tuple-ele, ...), custom_call_target="tpu_custom_call" | custom-call | tf_op jit(solution)/shard_map/finish/pallas_call | solution.py:421
Async XLA Ops:
  0.6 0.9 %copy-start = (f32[256,128]{1,0:T(8,128)S(1)}, f32[256,128]{1,0:T(8,128)}, u32[]{:S(2)}) copy-start(f32[256,128]{1,0:T(8,128)} %qm.1) | copy-start | bytes 393220
  1.6 0.9 %copy-start.1 = (f32[256,128]{1,0:T(8,128)S(1)}, f32[256,128]{1,0:T(8,128)}, u32[]{:S(2)}) copy-start(f32[256,128]{1,0:T(8,128)} %km.1) | copy-start | bytes 393220
  2.5 0.9 %copy-start.2 = (bf16[1024,128]{1,0:T(8,128)(2,1)S(1)}, bf16[1024,128]{1,0:T(8,128)(2,1)}, u32[]{:S(2)}) copy-start(bf16[1024,128]{1,0:T(8,128)(2,1)} %x_in.1) | copy-start | bytes 786436
  3.4 0.9 %copy-start.3 = (bf16[1024,128]{1,0:T(8,128)(2,1)S(1)}, bf16[1024,128]{1,0:T(8,128)(2,1)}, u32[]{:S(2)}) copy-start(bf16[1024,128]{1,0:T(8,128)(2,1)} %qc_in.1) | copy-start | bytes 786436
  4.4 0.9 %copy-start.4 = (bf16[1024,128]{1,0:T(8,128)(2,1)S(1)}, bf16[1024,128]{1,0:T(8,128)(2,1)}, u32[]{:S(2)}) copy-start(bf16[1024,128]{1,0:T(8,128)(2,1)} %kc_in.1) | copy-start | bytes 786436
  5.3 0.9 %copy-start.5 = (bf16[256,256]{1,0:T(8,128)(2,1)S(1)}, bf16[256,256]{1,0:T(8,128)(2,1)}, u32[]{:S(2)}) copy-start(bf16[256,256]{1,0:T(8,128)(2,1)} %qb_in.1) | copy-start | bytes 393220
  6.2 0.9 %copy-start.6 = (bf16[256,256]{1,0:T(8,128)(2,1)S(1)}, bf16[256,256]{1,0:T(8,128)(2,1)}, u32[]{:S(2)}) copy-start(bf16[256,256]{1,0:T(8,128)(2,1)} %kb_in.1) | copy-start | bytes 393220
  7.1 0.7 copy-start.7
  7.8 0.7 copy-start.8
  8.5 0.7 copy-start.9
  9.2 0.7 copy-start.10

commit v2 on v1

--- a/solution.py
+++ b/solution.py
@@ -26,6 +26,7 @@
 norm_floor = 0.01
 step_rate = 0.01
 
+VMEM_ALL = 67_043_328
 MESH_ID = pl.DeviceIdType.MESH
 BF = jnp.bfloat16
 F32 = jnp.float32
@@ -37,6 +38,18 @@
 ALONG_Z = [8, 7, -7, 6, -6, 5, -5, 4, -4, 3, -3, 2, -2, 1, -1]
 Z_FIRST = [6, -6, 3, -3, 1, -1]
 Z_RELAY = [(3, (1, -1)), (-3, (-1, 1)), (6, (2, 1, -1)), (-6, (-1, 1))]
+
+
+class Phases:
+    def __init__(self):
+        self.open = None
+
+    def __call__(self, name):
+        if self.open is not None:
+            self.open.__exit__(None, None, None)
+        self.open = jax.named_scope(name) if name else None
+        if self.open is not None:
+            self.open.__enter__()
 
 
 class Sends:
@@ -151,17 +164,19 @@
 
 def exchange(
     x_in, qc_in, kc_in, qm_in, km_in, qb_in, kb_in, qf_in, qs_in, kf_in, ks_in,
-    basis, masters, ratios, moments_out,
-    xs, xg, cots, cot_other, cot_rel, cot_t, mas, mom, mom_other,
+    basis_out, masters_out, ratios, moments_out,
+    basis, masters, xs, xg, cots, cot_other, cot_rel, cot_t, mas, mom, mom_other,
     psend, precv, xb, lowp, lowr, rsend, msend,
-    load_sem, send_sem, recv_sem,
+    load_sem, store_sem, send_sem, recv_sem,
 ):
     y, x, z, c = (lax.axis_index(a) for a in AXES)
     me = (y, x, z, c)
     oc = 1 - c
+    phase = Phases()
     f = y * XN + x
     partner = (y, x, z, oc)
 
+    phase("enter")
     barrier = pltpu.get_barrier_semaphore()
     near = [(wrap(y + dy, YN), wrap(x + dx, XN), z, c) for dy, dx in PLANE]
     near += [(wrap(y + dy, YN), wrap(x + dx, XN), z, oc) for dy, dx in PLANE]
@@ -189,14 +204,17 @@
     load(ks_in, mom.at[1, 1])
     load(qm_in, mas.at[0])
     load(km_in, mas.at[1])
+    phase("loads")
     for copy in loads:
         copy.wait()
     masters[f, :, 0:HD] = mas[0].astype(BF)
     masters[f, :, HD : 2 * HD] = mas[1].astype(BF)
 
     sends = Sends(send_sem, recv_sem)
+    phase("barrier")
     pl.semaphore_wait(barrier, len(near))
 
+    phase("send_inputs")
     def xslot(zz):
         return xg.at[:, pl.ds(pl.multiple_of(zz * HD, HD), HD)]
 
@@ -216,8 +234,10 @@
     sends.start(n_cot, cots.at[oc], cot_other, partner)
     sends.start(n_mom, mom.at[oc], mom_other, partner)
     xg[:, pl.ds(pl.multiple_of(z * HD, HD), HD)] = xs[pl.ds(pl.multiple_of(z * SUB, SUB), SUB), :]
+    phase("basis_1")
     next(gather_basis)
 
+    phase("cot_rel")
     sends.landed(n_cot, cot_other, partner)
     sends.landed(n_mom, mom_other, partner)
     for o in range(ZN):
@@ -225,15 +245,28 @@
         rows = pl.ds(pl.multiple_of(zz * SUB, SUB), SUB)
         cot_rel[o * SUB : (o + 1) * SUB, 0:HD] = cots[c, rows, :]
         cot_rel[o * SUB : (o + 1) * SUB, HD : 2 * HD] = cot_other[rows, :]
+    phase("basis_23")
     next(gather_basis)
     next(gather_basis)
+    phase("cot_t")
     cot_t[...] = cot_rel[...].T
+    phase("basis_rest")
     for _ in gather_basis:
         pass
+    stores = []
+
+    def store(src, dst):
+        copy = pltpu.make_async_copy(src, dst, store_sem.at[len(stores)])
+        copy.start()
+        stores.append(copy)
+
+    store(basis.at[:, c], basis_out.at[:, c])
+    phase("wait_x")
     next(gather_masters)
     for d in ALONG_Z:
         sends.landed(nx[d], xslot(wrap(z - d, ZN)), partner)
 
+    phase("xb")
     part = jnp.zeros((SUB, 2 * RANK), F32)
     for k in range(FN // 2):
         rows = basis[2 * k : 2 * k + 2, c].reshape(2 * HALF, 2 * RANK)
@@ -245,6 +278,7 @@
     n_part = sends.take()
     sends.start(n_part, psend.at[oc], precv, partner)
     n_basis = sends.take()
+    phase("d2d_part")
     sends.landed(n_part, precv, partner)
     xb[0] = (psend[c] + precv[...]).astype(BF)
 
@@ -266,36 +300,47 @@
             seen.add(o % ZN)
             sends.landed(nz[o % ZN], xb.at[o % ZN], partner)
 
+    phase("z_send")
     for d in Z_FIRST:
         z_send(0, d)
     sends.start(n_basis, basis.at[:, c], basis.at[:, c], partner)
     next(gather_masters)
+    phase("z_relay1")
     for o, hops in Z_RELAY[:2]:
         z_landed(o)
         for d in hops:
             z_send(o, d)
+    phase("z_relay2")
     for o, hops in Z_RELAY[2:]:
         z_landed(o)
         for d in hops:
             z_send(o, d)
+    phase("masters")
     next(gather_masters)
     next(gather_masters)
     next(gather_masters)
+    phase("z_rest")
     for o in range(1, ZN):
         z_landed(o)
-
+    sends.landed(n_basis, basis.at[:, oc], partner)
+    store(basis.at[:, oc], basis_out.at[:, oc])
+
+    phase("low")
     low_t = jnp.dot(cot_t[...], xb[...].reshape(TOK, RANK), preferred_element_type=F32)
     lowp[...] = low_t.T.reshape(FN, LOW, 2 * HD)
     nl = {p: sends.take() for p in PLANE}
     for dy, dx in PLANE:
         ty, tx = wrap(y + dy, YN), wrap(x + dx, XN)
         sends.start(nl[dy, dx], lowp.at[ty * XN + tx], lowr.at[dy * XN + dx], (ty, tx, z, c))
+    phase("low_m")
     next(gather_masters)
+    phase("low_recv")
     low = lowp[f]
     for dy, dx in PLANE:
         sends.landed(nl[dy, dx], lowr.at[dy * XN + dx], partner)
         low = low + lowr[dy * XN + dx]
 
+    phase("moments")
     nr = {(p, k): sends.take() for p in [(0, 0)] + PLANE for k in (0, 1)}
     n_out = sends.take()
     for k, (first, second) in enumerate(
@@ -319,9 +364,11 @@
                 continue
             sends.start(nr[(dy, dx), k], rsend.at[k], ratios.at[c, f], (ty, tx, z, core))
     sends.start(n_out, msend, moments_out.at[c], partner)
+    phase("masters_rest")
     for _ in gather_masters:
         pass
-    sends.landed(n_basis, basis.at[:, oc], partner)
+    store(masters, masters_out)
+    phase("ratio_recv")
     for dy, dx in PLANE + [(0, 0)]:
         sy, sx = wrap(y - dy, YN), wrap(x - dx, XN)
         for k in (0, 1):
@@ -329,50 +376,93 @@
                 continue
             m = c if k == 0 else oc
             sends.landed(nr[(dy, dx), k], ratios.at[m, sy * XN + sx], partner)
+    phase("fin")
     sends.landed(n_out, moments_out.at[oc], partner)
     sends.finish()
+    for copy in stores:
+        copy.wait()
+    phase(None)
 
 
 N_SENDS = 15 + 80 + 2 + 2 + 15 + 15 + 32 + 1
 
 
+GROUP = 4
+GROUPS = FN // GROUP
+
+
 def finish(
-    basis, masters, ratios, moments, qm, km,
+    basis_in, masters_in, ratios_in, moments_in, qm_in, km_in,
     q_step, q_weight, q_copy, q_first, q_second,
     k_step, k_weight, k_copy, k_first, k_second,
-    held,
+    basis, masters, ratios, moments, own, held, steps, weights, copies,
+    load_sem, store_sem,
 ):
     f = lax.axis_index("y") * XN + lax.axis_index("x")
-    outs = (
-        (qm, q_step, q_weight, q_copy, q_first, q_second),
-        (km, k_step, k_weight, k_copy, k_first, k_second),
-    )
-    for m, (master, step_ref, weight_ref, copy_ref, first_ref, second_ref) in enumerate(outs):
-        first_ref[...] = moments[m, 0]
-        second_ref[...] = moments[m, 1]
-        ratio = ratios[m].reshape(RANK, HD)
-
-        def product(k, total):
-            rows = basis[k, :, :, m * RANK : (m + 1) * RANK].reshape(ROWS, RANK)
-            update = jnp.dot(rows, ratio, preferred_element_type=F32)
-            held[k] = update
-            return total + jnp.sum((update * update).reshape(ROWS // 8, 8, HD), axis=0)
-
-        total = lax.fori_loop(0, FN, product, jnp.zeros((8, HD), F32), unroll=2)
-        scale = 1.0 / jnp.sqrt(jnp.sum(total) / (D * HD) + norm_floor)
-
-        def scaled(k, _):
-            step = held[k] * scale
-            old = masters[k, :, m * HD : (m + 1) * HD].astype(F32)
-            copy_ref[pl.ds(pl.multiple_of(k * ROWS, ROWS), ROWS), :] = (
-                old - step_rate * step
-            ).astype(BF)
-            return 0
-
-        lax.fori_loop(0, FN, scaled, 0)
-        step = held[f] * scale
-        step_ref[...] = step
-        weight_ref[...] = master[...] - step_rate * step
+    loads, stores = [], []
+    phase = Phases()
+
+    def load(src, dst):
+        copy = pltpu.make_async_copy(src, dst, load_sem.at[len(loads)])
+        copy.start()
+        loads.append(copy)
+        return copy
+
+    def store(src, dst):
+        copy = pltpu.make_async_copy(src, dst, store_sem.at[len(stores)])
+        copy.start()
+        stores.append(copy)
+
+    def group(g):
+        return pl.ds(g * GROUP, GROUP)
+
+    ratio_load = load(ratios_in, ratios)
+    basis_loads = [load(basis_in.at[group(g)], basis.at[group(g)]) for g in range(GROUPS)]
+    moments_load = load(moments_in, moments)
+    own_loads = [load(qm_in, own.at[0]), load(km_in, own.at[1])]
+    masters_loads = [load(masters_in.at[group(g)], masters.at[group(g)]) for g in range(GROUPS)]
+
+    phase("ratio_wait")
+    ratio_load.wait()
+    ratio = [ratios[m].reshape(RANK, HD) for m in range(2)]
+    phase("product")
+    totals = [jnp.zeros((8, HD), F32) for _ in range(2)]
+    for g in range(GROUPS):
+        basis_loads[g].wait()
+        for k in range(g * GROUP, (g + 1) * GROUP):
+            for m in range(2):
+                rows = basis[k, :, :, m * RANK : (m + 1) * RANK].reshape(ROWS, RANK)
+                update = jnp.dot(rows, ratio[m], preferred_element_type=F32)
+                held[m, k] = update
+                totals[m] += jnp.sum((update * update).reshape(ROWS // 8, 8, HD), axis=0)
+    phase("scale")
+    moments_load.wait()
+    for m, refs in enumerate(((q_first, q_second), (k_first, k_second))):
+        for i in range(2):
+            store(moments.at[m, i], refs[i])
+    scales = [1.0 / jnp.sqrt(jnp.sum(t) / (D * HD) + norm_floor) for t in totals]
+    for m, (step_ref, weight_ref) in enumerate(((q_step, q_weight), (k_step, k_weight))):
+        own_loads[m].wait()
+        step = held[m, f] * scales[m]
+        steps[m] = step
+        weights[m] = own[m] - step_rate * step
+        store(steps.at[m], step_ref)
+        store(weights.at[m], weight_ref)
+    phase("copies")
+    for g in range(GROUPS):
+        masters_loads[g].wait()
+        for m, copy_ref in enumerate((q_copy, k_copy)):
+            for k in range(g * GROUP, (g + 1) * GROUP):
+                old = masters[k, :, m * HD : (m + 1) * HD].astype(F32)
+                copies[m, k * ROWS : (k + 1) * ROWS] = (
+                    old - step_rate * (held[m, k] * scales[m])
+                ).astype(BF)
+            rows = pl.ds(g * GROUP * ROWS, GROUP * ROWS)
+            store(copies.at[m, rows], copy_ref.at[rows])
+    phase("drain")
+    for copy in stores:
+        copy.wait()
+    phase(None)
 
 
 def body(*args):
@@ -389,8 +479,10 @@
             jax.ShapeDtypeStruct((2, 2, LOW, HD), F32),
         ),
         in_specs=[any_space] * len(args),
-        out_specs=(vmem,) * 4,
+        out_specs=(any_space, any_space, vmem, vmem),
         scratch_shapes=[
+            pltpu.VMEM((FN, CN, HALF, 2 * RANK), BF),
+            pltpu.VMEM((FN, ROWS, 2 * HD), BF),
             pltpu.VMEM((TOK, HD), BF),
             pltpu.VMEM((SUB, ZN * HD), BF),
             pltpu.VMEM((2, TOK, HD), BF),
@@ -408,11 +500,12 @@
             pltpu.VMEM((2, LOW, HD), BF),
             pltpu.VMEM((2, LOW, HD), F32),
             dma((11,)),
+            dma((3,)),
             dma((N_SENDS,)),
             dma((N_SENDS,)),
         ],
         compiler_params=pltpu.CompilerParams(
-            collective_id=0, has_side_effects=True, vmem_limit_bytes=48 * 1024 * 1024
+            collective_id=0, has_side_effects=True, vmem_limit_bytes=VMEM_ALL
         ),
     )(*args)
     matrix = jax.ShapeDtypeStruct((ROWS, HD), F32)
@@ -422,10 +515,22 @@
         finish,
         name="finish",
         out_shape=(matrix, matrix, whole, moment, moment) * 2,
-        in_specs=[vmem] * 6,
-        out_specs=(vmem,) * 10,
-        scratch_shapes=[pltpu.VMEM((FN, ROWS, HD), F32)],
-        compiler_params=pltpu.CompilerParams(vmem_limit_bytes=48 * 1024 * 1024),
+        in_specs=[any_space] * 6,
+        out_specs=(any_space,) * 10,
+        scratch_shapes=[
+            pltpu.VMEM((FN, CN, HALF, 2 * RANK), BF),
+            pltpu.VMEM((FN, ROWS, 2 * HD), BF),
+            pltpu.VMEM((2, FN, LOW, HD), BF),
+            pltpu.VMEM((2, 2, LOW, HD), F32),
+            pltpu.VMEM((2, ROWS, HD), F32),
+            pltpu.VMEM((2, FN, ROWS, HD), F32),
+            pltpu.VMEM((2, ROWS, HD), F32),
+            pltpu.VMEM((2, ROWS, HD), F32),
+            pltpu.VMEM((2, D, HD), BF),
+            dma((4 + 2 * GROUPS,)),
+            dma((8 + 2 * GROUPS,)),
+        ],
+        compiler_params=pltpu.CompilerParams(vmem_limit_bytes=VMEM_ALL),
     )(basis, masters, ratios, moments, args[3], args[4])
 
 

time: 85.1 us -> 70.9 us (0.83)
  local copies, waits for them, and re-layouts: 9.24 us -> 0 us
  Pallas kernels: 74.7 us -> 70.1 us
    unnamed x22 -> x0, local copies, waits for them, and re-layouts: 9.24 us -> none
    pallas_call x1, Pallas kernels: 8.35 us -> 5.02 us  [body(): pl.pallas_call(finish, name='finish', out_shape=(matrix, matrix, whole, m...]
    pallas_call x1, Pallas kernels: 66.3 us -> 65.1 us  [body(): pl.pallas_call(exchange, name='exchange', out_shape=(jax.ShapeDtypeStruct...]
where the time goes in v2:
time: 70.9 us; the launch traced here: 70.7 us
  Pallas kernels  70.1 us (99%)
    pallas_call x1, Pallas kernels, body(): pl.pallas_call(exchange, name='exchange', out_shape=(jax.ShapeDtypeStruct...  65.1 us
    pallas_call x1, Pallas kernels, body(): pl.pallas_call(finish, name='finish', out_shape=(matrix, matrix, whole, m...  5.02 us

profile of v2, /device:TPU:1, one launch (start us, length us, event | category | flops | bytes accessed | tf_op | source)
XLA Modules:
  0.0 70.7 jit_solution(17940774355859175006)
XLA Ops:
  0.6 65.1 %exchange.1 = (bf16[16,2,128,512]{3,2,1,0:T(8,128)(2,1)}, bf16[16,256,256]{2,1,0:T(8,128)(2,1)}, bf16[2,16,16,128]{3,2,1,0:T(8,128)(2,1)}, f32[2,2,16,128]{3,2,1,0:T(8,128)}) custom-call(bf16[1024,128]{1,0:T(8,128)(2,1)} %x_in.1, bf16[1024,128]{1,0:T(8,128)(2,1)} %qc_in.1, bf16[1024,128]{1,0:T(8,128)(2,1)} %kc_in.1, f32[256,128]{1,0:T(8,128)} %qm_in.3, ...), custom_call_target="tpu_custom_call" | custom-call | tf_op jit(solution)/shard_map/exchange/pallas_call | solution.py:472
  65.7 5.0 %finish.1 = (f32[256,128]{1,0:T(8,128)}, f32[256,128]{1,0:T(8,128)}, bf16[4096,128]{1,0:T(8,128)(2,1)}, f32[16,128]{1,0:T(8,128)}, f32[16,128]{1,0:T(8,128)}, /*...) custom-call(bf16[16,2,128,512]{3,2,1,0:T(8,128)(2,1)} %get-tuple-ele, ...), custom_call_target="tpu_custom_call" | custom-call | tf_op jit(solution)/shard_map/finish/pallas_call | solution.py:514

commit v3 on v2

--- a/solution.py
+++ b/solution.py
@@ -26,7 +26,7 @@
 norm_floor = 0.01
 step_rate = 0.01
 
-VMEM_ALL = 67_043_328
+VMEM_GRANT = 20 * 1024 * 1024
 MESH_ID = pl.DeviceIdType.MESH
 BF = jnp.bfloat16
 F32 = jnp.float32
@@ -164,10 +164,10 @@
 
 def exchange(
     x_in, qc_in, kc_in, qm_in, km_in, qb_in, kb_in, qf_in, qs_in, kf_in, ks_in,
-    basis_out, masters_out, ratios, moments_out,
-    basis, masters, xs, xg, cots, cot_other, cot_rel, cot_t, mas, mom, mom_other,
+    basis, masters, ratios, moments_out, mas,
+    xs, xg, cots, cot_other, cot_rel, cot_t, mom, mom_other,
     psend, precv, xb, lowp, lowr, rsend, msend,
-    load_sem, store_sem, send_sem, recv_sem,
+    load_sem, send_sem, recv_sem,
 ):
     y, x, z, c = (lax.axis_index(a) for a in AXES)
     me = (y, x, z, c)
@@ -253,14 +253,6 @@
     phase("basis_rest")
     for _ in gather_basis:
         pass
-    stores = []
-
-    def store(src, dst):
-        copy = pltpu.make_async_copy(src, dst, store_sem.at[len(stores)])
-        copy.start()
-        stores.append(copy)
-
-    store(basis.at[:, c], basis_out.at[:, c])
     phase("wait_x")
     next(gather_masters)
     for d in ALONG_Z:
@@ -323,7 +315,6 @@
     for o in range(1, ZN):
         z_landed(o)
     sends.landed(n_basis, basis.at[:, oc], partner)
-    store(basis.at[:, oc], basis_out.at[:, oc])
 
     phase("low")
     low_t = jnp.dot(cot_t[...], xb[...].reshape(TOK, RANK), preferred_element_type=F32)
@@ -367,7 +358,6 @@
     phase("masters_rest")
     for _ in gather_masters:
         pass
-    store(masters, masters_out)
     phase("ratio_recv")
     for dy, dx in PLANE + [(0, 0)]:
         sy, sx = wrap(y - dy, YN), wrap(x - dx, XN)
@@ -379,8 +369,6 @@
     phase("fin")
     sends.landed(n_out, moments_out.at[oc], partner)
     sends.finish()
-    for copy in stores:
-        copy.wait()
     phase(None)
 
 
@@ -392,43 +380,25 @@
 
 
 def finish(
-    basis_in, masters_in, ratios_in, moments_in, qm_in, km_in,
+    basis, masters, ratios, moments, own,
     q_step, q_weight, q_copy, q_first, q_second,
     k_step, k_weight, k_copy, k_first, k_second,
-    basis, masters, ratios, moments, own, held, steps, weights, copies,
-    load_sem, store_sem,
+    held, steps, weights, copies,
+    store_sem,
 ):
     f = lax.axis_index("y") * XN + lax.axis_index("x")
-    loads, stores = [], []
+    stores = []
     phase = Phases()
-
-    def load(src, dst):
-        copy = pltpu.make_async_copy(src, dst, load_sem.at[len(loads)])
-        copy.start()
-        loads.append(copy)
-        return copy
 
     def store(src, dst):
         copy = pltpu.make_async_copy(src, dst, store_sem.at[len(stores)])
         copy.start()
         stores.append(copy)
 
-    def group(g):
-        return pl.ds(g * GROUP, GROUP)
-
-    ratio_load = load(ratios_in, ratios)
-    basis_loads = [load(basis_in.at[group(g)], basis.at[group(g)]) for g in range(GROUPS)]
-    moments_load = load(moments_in, moments)
-    own_loads = [load(qm_in, own.at[0]), load(km_in, own.at[1])]
-    masters_loads = [load(masters_in.at[group(g)], masters.at[group(g)]) for g in range(GROUPS)]
-
-    phase("ratio_wait")
-    ratio_load.wait()
+    phase("product")
     ratio = [ratios[m].reshape(RANK, HD) for m in range(2)]
-    phase("product")
     totals = [jnp.zeros((8, HD), F32) for _ in range(2)]
     for g in range(GROUPS):
-        basis_loads[g].wait()
         for k in range(g * GROUP, (g + 1) * GROUP):
             for m in range(2):
                 rows = basis[k, :, :, m * RANK : (m + 1) * RANK].reshape(ROWS, RANK)
@@ -436,13 +406,11 @@
                 held[m, k] = update
                 totals[m] += jnp.sum((update * update).reshape(ROWS // 8, 8, HD), axis=0)
     phase("scale")
-    moments_load.wait()
     for m, refs in enumerate(((q_first, q_second), (k_first, k_second))):
         for i in range(2):
             store(moments.at[m, i], refs[i])
     scales = [1.0 / jnp.sqrt(jnp.sum(t) / (D * HD) + norm_floor) for t in totals]
     for m, (step_ref, weight_ref) in enumerate(((q_step, q_weight), (k_step, k_weight))):
-        own_loads[m].wait()
         step = held[m, f] * scales[m]
         steps[m] = step
         weights[m] = own[m] - step_rate * step
@@ -450,7 +418,6 @@
         store(weights.at[m], weight_ref)
     phase("copies")
     for g in range(GROUPS):
-        masters_loads[g].wait()
         for m, copy_ref in enumerate((q_copy, k_copy)):
             for k in range(g * GROUP, (g + 1) * GROUP):
                 old = masters[k, :, m * HD : (m + 1) * HD].astype(F32)
@@ -466,10 +433,10 @@
 
 
 def body(*args):
-    any_space = pl.BlockSpec(memory_space=pl.ANY)
+    hbm = pl.BlockSpec(memory_space=pltpu.HBM)
     vmem = pl.BlockSpec(memory_space=pltpu.VMEM)
     dma = pltpu.SemaphoreType.DMA
-    basis, masters, ratios, moments = pl.pallas_call(
+    handed = pl.pallas_call(
         exchange,
         name="exchange",
         out_shape=(
@@ -477,19 +444,17 @@
             jax.ShapeDtypeStruct((FN, ROWS, 2 * HD), BF),
             jax.ShapeDtypeStruct((2, FN, LOW, HD), BF),
             jax.ShapeDtypeStruct((2, 2, LOW, HD), F32),
+            jax.ShapeDtypeStruct((2, ROWS, HD), F32),
         ),
-        in_specs=[any_space] * len(args),
-        out_specs=(any_space, any_space, vmem, vmem),
+        in_specs=[hbm] * len(args),
+        out_specs=(vmem,) * 5,
         scratch_shapes=[
-            pltpu.VMEM((FN, CN, HALF, 2 * RANK), BF),
-            pltpu.VMEM((FN, ROWS, 2 * HD), BF),
             pltpu.VMEM((TOK, HD), BF),
             pltpu.VMEM((SUB, ZN * HD), BF),
             pltpu.VMEM((2, TOK, HD), BF),
             pltpu.VMEM((TOK, HD), BF),
             pltpu.VMEM((TOK, 2 * HD), BF),
             pltpu.VMEM((2 * HD, TOK), BF),
-            pltpu.VMEM((2, ROWS, HD), F32),
             pltpu.VMEM((2, 2, LOW, HD), F32),
             pltpu.VMEM((2, LOW, HD), F32),
             pltpu.VMEM((2, SUB, RANK), F32),
@@ -500,14 +465,13 @@
             pltpu.VMEM((2, LOW, HD), BF),
             pltpu.VMEM((2, LOW, HD), F32),
             dma((11,)),
-            dma((3,)),
             dma((N_SENDS,)),
             dma((N_SENDS,)),
         ],
         compiler_params=pltpu.CompilerParams(
-            collective_id=0, has_side_effects=True, vmem_limit_bytes=VMEM_ALL
+            collective_id=0, has_side_effects=True, vmem_limit_bytes=VMEM_GRANT
         ),
-    )(*args)
+    )(*(pltpu.with_memory_space_constraint(a, pltpu.HBM) for a in args))
     matrix = jax.ShapeDtypeStruct((ROWS, HD), F32)
     whole = jax.ShapeDtypeStruct((D, HD), BF)
     moment = jax.ShapeDtypeStruct((LOW, HD), F32)
@@ -515,23 +479,17 @@
         finish,
         name="finish",
         out_shape=(matrix, matrix, whole, moment, moment) * 2,
-        in_specs=[any_space] * 6,
-        out_specs=(any_space,) * 10,
+        in_specs=[vmem] * 5,
+        out_specs=(hbm,) * 10,
         scratch_shapes=[
-            pltpu.VMEM((FN, CN, HALF, 2 * RANK), BF),
-            pltpu.VMEM((FN, ROWS, 2 * HD), BF),
-            pltpu.VMEM((2, FN, LOW, HD), BF),
-            pltpu.VMEM((2, 2, LOW, HD), F32),
-            pltpu.VMEM((2, ROWS, HD), F32),
             pltpu.VMEM((2, FN, ROWS, HD), F32),
             pltpu.VMEM((2, ROWS, HD), F32),
             pltpu.VMEM((2, ROWS, HD), F32),
             pltpu.VMEM((2, D, HD), BF),
-            dma((4 + 2 * GROUPS,)),
             dma((8 + 2 * GROUPS,)),
         ],
-        compiler_params=pltpu.CompilerParams(vmem_limit_bytes=VMEM_ALL),
-    )(basis, masters, ratios, moments, args[3], args[4])
+        compiler_params=pltpu.CompilerParams(vmem_limit_bytes=VMEM_GRANT),
+    )(*handed)
 
 
 def solution(mesh):

time: 70.9 us -> 68.3 us (0.963)
  Pallas kernels: 70.1 us -> 67.5 us
    pallas_call x1, Pallas kernels: 5.02 us -> 3.08 us  [body(): pl.pallas_call(finish, name='finish', out_shape=(matrix, matrix, whole, m...]
where the time goes in v3:
time: 68.3 us; the launch traced here: 68.1 us
  Pallas kernels  67.5 us (99%)
    pallas_call x1, Pallas kernels, body(): pl.pallas_call(exchange, name='exchange', out_shape=(jax.ShapeDtypeStruct...  64.4 us
    pallas_call x1, Pallas kernels, body(): pl.pallas_call(finish, name='finish', out_shape=(matrix, matrix, whole, m...  3.08 us

profile of v3, /device:TPU:1, one launch (start us, length us, event | category | flops | bytes accessed | tf_op | source)
XLA Modules:
  0.0 68.1 jit_solution(11162463915442833356)
XLA Ops:
  0.6 64.4 %exchange.1 = (bf16[16,2,128,512]{3,2,1,0:T(8,128)(2,1)S(1)}, bf16[16,256,256]{2,1,0:T(8,128)(2,1)S(1)}, bf16[2,16,16,128]{3,2,1,0:T(8,128)(2,1)S(1)}, f32[2,2,16,128]{3,2,1,0:T(8,128)S(1)}, f32[2,256,128]{2,1,0:T(8,128)S(1)}) custom-call(bf16[1024,128]{1,0:T(8,128)(2,1)} %x_in.1, bf16[1024,128]{1,0:T(8,128)(2,1)} %qc_in.1, bf16[1024,128]{1,0:T(8,128)(2,1)} %kc_in.1, ...), custom_call_target="tpu_custom_call" | custom-call | tf_op jit(solution)/shard_map/exchange/pallas_call | solution.py:439
  65.0 3.1 %finish.1 = (f32[256,128]{1,0:T(8,128)}, f32[256,128]{1,0:T(8,128)}, bf16[4096,128]{1,0:T(8,128)(2,1)}, f32[16,128]{1,0:T(8,128)}, f32[16,128]{1,0:T(8,128)}, /*...) custom-call(bf16[16,2,128,512]{3,2,1,0:T(8,128)(2,1)S(1)} %get-tuple, ...), custom_call_target="tpu_custom_call" | custom-call | tf_op jit(solution)/shard_map/finish/pallas_call | solution.py:478

commit v4 on v3

--- a/solution.py
+++ b/solution.py
@@ -55,45 +55,51 @@
 class Sends:
     def __init__(self, send_sem, recv_sem):
         self.send_sem, self.recv_sem = send_sem, recv_sem
-        self.count = 0
-        self.started = []
-
-    def take(self):
-        self.count += 1
-        return self.count - 1
-
-    def start(self, number, src, dst, device):
-        copy = pltpu.make_async_remote_copy(
+        self.sent = self.received = 0
+        self.open = []
+
+    def sent_group(self, whole):
+        self.open.append((self.sent, whole))
+        self.sent += 1
+        return self.sent - 1
+
+    def received_group(self):
+        self.received += 1
+        return self.received - 1
+
+    def start(self, sent, received, src, dst, device):
+        pltpu.make_async_remote_copy(
             src_ref=src,
             dst_ref=dst,
-            send_sem=self.send_sem.at[number],
-            recv_sem=self.recv_sem.at[number],
+            send_sem=self.send_sem.at[sent],
+            recv_sem=self.recv_sem.at[received],
+            device_id=device,
+            device_id_type=MESH_ID,
+        ).start()
+
+    def whole(self, sent, received, ref, device):
+        return pltpu.make_async_remote_copy(
+            src_ref=ref,
+            dst_ref=ref,
+            send_sem=self.send_sem.at[sent],
+            recv_sem=self.recv_sem.at[received],
             device_id=device,
             device_id_type=MESH_ID,
         )
-        copy.start()
-        self.started.append(copy)
-
-    def landed(self, number, dst, device):
-        pltpu.make_async_remote_copy(
-            src_ref=dst,
-            dst_ref=dst,
-            send_sem=self.send_sem.at[number],
-            recv_sem=self.recv_sem.at[number],
-            device_id=device,
-            device_id_type=MESH_ID,
-        ).wait_recv()
-
-    def finish(self):
-        for copy in self.started:
-            copy.wait_send()
+
+    def landed(self, received, ref, device):
+        self.whole(0, received, ref, device).wait_recv()
+
+    def finish(self, device):
+        for group, ref in self.open:
+            self.whole(group, 0, ref, device).wait_send()
 
 
 def wrap(value, count):
     return lax.rem(value + 2 * count, count)
 
 
-def plane_gather(sends, piece, me, rows):
+def plane_gather(sends, piece, many, me, rows):
     y, x, z, c = me
     half, quarter = rows // 2, rows // 4
     signs = (1, -1)
@@ -113,60 +119,62 @@
         return (fy, fx, z, c)
 
     part_of = {1: 0, -1: 1}
-    both = [(h, s) for h in (0, 1) for s in signs]
-    n1 = {k: sends.take() for k in both}
-    n1r = {k: sends.take() for k in both}
-    n2 = {(h, j, s): sends.take() for j in (0, -1, 1, 2) for h, s in both}
-    n2r = {(h, j, s): sends.take() for j in (0, -1, 1, 2) for h, s in both}
+    halves = (0, 1)
+    sent = sends.sent_group(many(FN - 1, 0, rows))
+    n1 = {h: sends.received_group() for h in halves}
+    n1r = {h: sends.received_group() for h in halves}
+    n2 = {(h, j): sends.received_group() for j in (0, -1, 1, 2) for h in halves}
+    n2r = sends.received_group()
+    me_dev = dev(0, 1, 0)
+
+    def go(number, source, target):
+        sends.start(sent, number, source, source, target)
 
     def second_stage(h, j):
         for s in signs:
-            sends.start(n2[h, j, s], ref(h, j, 0), ref(h, j, 0), dev(h, 0, s))
+            go(n2[h, j], ref(h, j, 0), dev(h, 0, s))
 
     def second_relay(h, j):
+        sends.landed(n2[h, j], many(2, 0, half), me_dev)
         for s in signs:
-            sends.landed(n2[h, j, s], ref(h, j, -s), dev(h, 0, s))
-            p = part_of[s]
-            sends.start(n2r[h, j, s], ref(h, j, -s, p), ref(h, j, -s, p), dev(h, 0, s))
-
-    for h, s in both:
-        sends.start(n1[h, s], ref(h, 0, 0), ref(h, 0, 0), dev(h, s, 0))
-    for h in (0, 1):
+            go(n2r, ref(h, j, -s, part_of[s]), dev(h, 0, s))
+
+    for h in halves:
+        for s in signs:
+            go(n1[h], ref(h, 0, 0), dev(h, s, 0))
+    for h in halves:
         second_stage(h, 0)
     yield
-    for h, s in both:
-        sends.landed(n1[h, s], ref(h, -s, 0), dev(h, s, 0))
-        p = part_of[s]
-        sends.start(n1r[h, s], ref(h, -s, 0, p), ref(h, -s, 0, p), dev(h, s, 0))
-        second_stage(h, -s)
+    for h in halves:
+        sends.landed(n1[h], many(2, 0, half), me_dev)
+        for s in signs:
+            go(n1r[h], ref(h, -s, 0, part_of[s]), dev(h, s, 0))
+    for h in halves:
+        second_stage(h, -1)
+        second_stage(h, 1)
     yield
-    for h in (0, 1):
+    for h in halves:
         second_relay(h, 0)
     yield
-    for h in (0, 1):
-        for s in signs:
-            p = part_of[s]
-            sends.landed(n1r[h, s], ref(h, 2, 0, p), dev(h, s, 0))
+    for h in halves:
+        sends.landed(n1r[h], many(1, 0, half), me_dev)
         second_stage(h, 2)
     yield
     for j in (-1, 1):
-        for h in (0, 1):
+        for h in halves:
             second_relay(h, j)
     yield
-    for h in (0, 1):
+    for h in halves:
         second_relay(h, 2)
     yield
-    for j in (0, -1, 1, 2):
-        for h, s in both:
-            p = part_of[s]
-            sends.landed(n2r[h, j, s], ref(h, j, 2, p), dev(h, s, 0))
+    sends.landed(n2r, many(8, 0, half), me_dev)
 
 
 def exchange(
     x_in, qc_in, kc_in, qm_in, km_in, qb_in, kb_in, qf_in, qs_in, kf_in, ks_in,
     basis, masters, ratios, moments_out, mas,
     xs, xg, cots, cot_other, cot_rel, cot_t, mom, mom_other,
-    psend, precv, xb, lowp, lowr, rsend, msend,
+    psend, precv, xb, lowf, lowp, lowr, rsend, msend,
     load_sem, send_sem, recv_sem,
 ):
     y, x, z, c = (lax.axis_index(a) for a in AXES)
@@ -218,21 +226,35 @@
     def xslot(zz):
         return xg.at[:, pl.ds(pl.multiple_of(zz * HD, HD), HD)]
 
-    nx = {d: sends.take() for d in ALONG_Z}
+    several = xs.at[pl.ds(0, (ZN - 1) * SUB)]
+    sent_x, got_x = sends.sent_group(several), sends.received_group()
     gather_basis = plane_gather(
-        sends, lambda fy, fx, s, n: basis.at[fy * XN + fx, c, pl.ds(s, n)], me, HALF
+        sends,
+        lambda fy, fx, s, n: basis.at[fy * XN + fx, c, pl.ds(s, n)],
+        lambda k, s, n: basis.at[pl.ds(0, k), 0, pl.ds(s, n)],
+        me,
+        HALF,
     )
     gather_masters = plane_gather(
-        sends, lambda fy, fx, s, n: masters.at[fy * XN + fx, pl.ds(s, n)], me, ROWS
+        sends,
+        lambda fy, fx, s, n: masters.at[fy * XN + fx, pl.ds(s, n)],
+        lambda k, s, n: masters.at[pl.ds(0, k), pl.ds(s, n)],
+        me,
+        ROWS,
     )
     next(gather_basis)
     for d in ALONG_Z:
         zz = wrap(z + d, ZN)
         rows = xs.at[pl.ds(pl.multiple_of(zz * SUB, SUB), SUB)]
-        sends.start(nx[d], rows, xslot(z), (y, x, zz, c))
-    n_cot, n_mom = sends.take(), sends.take()
-    sends.start(n_cot, cots.at[oc], cot_other, partner)
-    sends.start(n_mom, mom.at[oc], mom_other, partner)
+        sends.start(sent_x, got_x, rows, xslot(z), (y, x, zz, c))
+
+    def swap(src, dst):
+        received = sends.received_group()
+        sends.start(sends.sent_group(src), received, src, dst, partner)
+        return received
+
+    n_cot = swap(cots.at[oc], cot_other)
+    n_mom = swap(mom.at[oc], mom_other)
     xg[:, pl.ds(pl.multiple_of(z * HD, HD), HD)] = xs[pl.ds(pl.multiple_of(z * SUB, SUB), SUB), :]
     phase("basis_1")
     next(gather_basis)
@@ -255,8 +277,7 @@
         pass
     phase("wait_x")
     next(gather_masters)
-    for d in ALONG_Z:
-        sends.landed(nx[d], xslot(wrap(z - d, ZN)), partner)
+    sends.landed(got_x, several, partner)
 
     phase("xb")
     part = jnp.zeros((SUB, 2 * RANK), F32)
@@ -267,35 +288,31 @@
         )
     psend[0] = part[:, :RANK]
     psend[1] = part[:, RANK:]
-    n_part = sends.take()
-    sends.start(n_part, psend.at[oc], precv, partner)
-    n_basis = sends.take()
+    n_part = swap(psend.at[oc], precv)
     phase("d2d_part")
     sends.landed(n_part, precv, partner)
     xb[0] = (psend[c] + precv[...]).astype(BF)
 
-    nz = {}
-    for d in Z_FIRST:
-        nz[d % ZN] = sends.take()
-    for o, hops in Z_RELAY:
-        for d in hops:
-            nz[(o + d) % ZN] = sends.take()
-    seen = set()
+    sent_z = sends.sent_group(xb.at[pl.ds(0, ZN - 1)])
+    nz = {o % ZN: sends.received_group() for o, _ in Z_RELAY}
+    rest_z = sends.received_group()
 
     def z_send(o, d):
         sends.start(
-            nz[(o + d) % ZN], xb.at[o % ZN], xb.at[(o + d) % ZN], (y, x, wrap(z + d, ZN), c)
+            sent_z,
+            nz.get((o + d) % ZN, rest_z),
+            xb.at[o % ZN],
+            xb.at[(o + d) % ZN],
+            (y, x, wrap(z + d, ZN), c),
         )
 
     def z_landed(o):
-        if o % ZN not in seen:
-            seen.add(o % ZN)
-            sends.landed(nz[o % ZN], xb.at[o % ZN], partner)
+        sends.landed(nz[o % ZN], xb.at[o % ZN], partner)
 
     phase("z_send")
     for d in Z_FIRST:
         z_send(0, d)
-    sends.start(n_basis, basis.at[:, c], basis.at[:, c], partner)
+    n_basis = swap(basis.at[:, c], basis.at[:, c])
     next(gather_masters)
     phase("z_relay1")
     for o, hops in Z_RELAY[:2]:
@@ -312,28 +329,29 @@
     next(gather_masters)
     next(gather_masters)
     phase("z_rest")
-    for o in range(1, ZN):
-        z_landed(o)
+    sends.landed(rest_z, xb.at[pl.ds(0, ZN - 1 - len(nz))], partner)
     sends.landed(n_basis, basis.at[:, oc], partner)
 
     phase("low")
     low_t = jnp.dot(cot_t[...], xb[...].reshape(TOK, RANK), preferred_element_type=F32)
-    lowp[...] = low_t.T.reshape(FN, LOW, 2 * HD)
-    nl = {p: sends.take() for p in PLANE}
+    lowf[...] = low_t.T.reshape(FN, LOW, 2 * HD)
+    lowp[...] = lowf[...].astype(BF)
+    all_low = lowr.at[pl.ds(1, FN - 1)]
+    sent_low, got_low = sends.sent_group(all_low), sends.received_group()
     for dy, dx in PLANE:
         ty, tx = wrap(y + dy, YN), wrap(x + dx, XN)
-        sends.start(nl[dy, dx], lowp.at[ty * XN + tx], lowr.at[dy * XN + dx], (ty, tx, z, c))
+        sends.start(sent_low, got_low, lowp.at[ty * XN + tx], lowr.at[dy * XN + dx], (ty, tx, z, c))
     phase("low_m")
     next(gather_masters)
     phase("low_recv")
-    low = lowp[f]
-    for dy, dx in PLANE:
-        sends.landed(nl[dy, dx], lowr.at[dy * XN + dx], partner)
-        low = low + lowr[dy * XN + dx]
+    low = lowf[f]
+    sends.landed(got_low, all_low, partner)
+    for k in range(1, FN):
+        low = low + lowr[k].astype(F32)
 
     phase("moments")
-    nr = {(p, k): sends.take() for p in [(0, 0)] + PLANE for k in (0, 1)}
-    n_out = sends.take()
+    all_ratios = xs.at[pl.ds(0, (2 * FN - 1) * LOW)]
+    sent_r, got_r = sends.sent_group(all_ratios), sends.received_group()
     for k, (first, second) in enumerate(
         ((mom[c, 0], mom[c, 1]), (mom_other[0], mom_other[1]))
     ):
@@ -353,26 +371,21 @@
         for k, core in ((0, c), (1, oc)):
             if k == 0 and (dy, dx) == (0, 0):
                 continue
-            sends.start(nr[(dy, dx), k], rsend.at[k], ratios.at[c, f], (ty, tx, z, core))
-    sends.start(n_out, msend, moments_out.at[c], partner)
+            sends.start(sent_r, got_r, rsend.at[k], ratios.at[c, f], (ty, tx, z, core))
+    n_out = swap(msend, moments_out.at[c])
     phase("masters_rest")
     for _ in gather_masters:
         pass
     phase("ratio_recv")
-    for dy, dx in PLANE + [(0, 0)]:
-        sy, sx = wrap(y - dy, YN), wrap(x - dx, XN)
-        for k in (0, 1):
-            if k == 0 and (dy, dx) == (0, 0):
-                continue
-            m = c if k == 0 else oc
-            sends.landed(nr[(dy, dx), k], ratios.at[m, sy * XN + sx], partner)
+    sends.landed(got_r, all_ratios, partner)
     phase("fin")
     sends.landed(n_out, moments_out.at[oc], partner)
-    sends.finish()
+    sends.finish(partner)
+    assert sends.sent <= N_SENT and sends.received <= N_RECEIVED
     phase(None)
 
 
-N_SENDS = 15 + 80 + 2 + 2 + 15 + 15 + 32 + 1
+N_SENT, N_RECEIVED = 11, 43
 
 
 GROUP = 4
@@ -461,12 +474,13 @@
             pltpu.VMEM((SUB, RANK), F32),
             pltpu.VMEM((ZN, SUB, RANK), BF),
             pltpu.VMEM((FN, LOW, 2 * HD), F32),
-            pltpu.VMEM((FN, LOW, 2 * HD), F32),
+            pltpu.VMEM((FN, LOW, 2 * HD), BF),
+            pltpu.VMEM((FN, LOW, 2 * HD), BF),
             pltpu.VMEM((2, LOW, HD), BF),
             pltpu.VMEM((2, LOW, HD), F32),
             dma((11,)),
-            dma((N_SENDS,)),
-            dma((N_SENDS,)),
+            dma((N_SENT,)),
+            dma((N_RECEIVED,)),
         ],
         compiler_params=pltpu.CompilerParams(
             collective_id=0, has_side_effects=True, vmem_limit_bytes=VMEM_GRANT

time: 68.3 us -> 62.9 us (0.921)
  Pallas kernels: 67.5 us -> 62.1 us
    pallas_call x1, Pallas kernels: 64.4 us -> 59 us  [body(): pl.pallas_call(exchange, name='exchange', out_shape=(jax.ShapeDtypeStruct...]
where the time goes in v4:
time: 62.9 us; the launch traced here: 62.8 us
  Pallas kernels  62.1 us (99%)
  between operations  0.65 us (1%)
    pallas_call x1, Pallas kernels, body(): pl.pallas_call(exchange, name='exchange', out_shape=(jax.ShapeDtypeStruct...  59 us
    pallas_call x1, Pallas kernels, body(): pl.pallas_call(finish, name='finish', out_shape=(matrix, matrix, whole, m...  3.08 us

profile of v4, /device:TPU:1, one launch (start us, length us, event | category | flops | bytes accessed | tf_op | source)
XLA Modules:
  0.0 62.8 jit_solution(15718023350037754498)
XLA Ops:
  0.6 59.0 %exchange.1 = (bf16[16,2,128,512]{3,2,1,0:T(8,128)(2,1)S(1)}, bf16[16,256,256]{2,1,0:T(8,128)(2,1)S(1)}, bf16[2,16,16,128]{3,2,1,0:T(8,128)(2,1)S(1)}, f32[2,2,16,128]{3,2,1,0:T(8,128)S(1)}, f32[2,256,128]{2,1,0:T(8,128)S(1)}) custom-call(bf16[1024,128]{1,0:T(8,128)(2,1)} %x_in.1, bf16[1024,128]{1,0:T(8,128)(2,1)} %qc_in.1, bf16[1024,128]{1,0:T(8,128)(2,1)} %kc_in.1, ...), custom_call_target="tpu_custom_call" | custom-call | tf_op jit(solution)/shard_map/exchange/pallas_call | solution.py:452
  59.7 3.1 %finish.1 = (f32[256,128]{1,0:T(8,128)}, f32[256,128]{1,0:T(8,128)}, bf16[4096,128]{1,0:T(8,128)(2,1)}, f32[16,128]{1,0:T(8,128)}, f32[16,128]{1,0:T(8,128)}, /*...) custom-call(bf16[16,2,128,512]{3,2,1,0:T(8,128)(2,1)S(1)} %get-tuple, ...), custom_call_target="tpu_custom_call" | custom-call | tf_op jit(solution)/shard_map/finish/pallas_call | solution.py:492

commit v5 on v4

--- a/solution.py
+++ b/solution.py
@@ -16,6 +16,8 @@
 ROWS = D // FN
 HALF = ROWS // CN
 LOW = RANK // FN
+CUTS = 2
+CUT = SUB // CUTS
 AXES = ("y", "x", "z", "c")
 FS = ("y", "x")
 TP = ("z", "c")
@@ -36,8 +38,8 @@
     key=lambda o: -(min(o[0], 4 - o[0]) + min(o[1], 4 - o[1])),
 )
 ALONG_Z = [8, 7, -7, 6, -6, 5, -5, 4, -4, 3, -3, 2, -2, 1, -1]
-Z_FIRST = [6, -6, 3, -3, 1, -1]
-Z_RELAY = [(3, (1, -1)), (-3, (-1, 1)), (6, (2, 1, -1)), (-6, (-1, 1))]
+Z_FIRST = [5, -5, 2, -2, 1, -1]
+Z_RELAY = [(5, (3, 2, 1, -1)), (-5, (-2, -1, 1)), (2, (1,)), (-2, (-1,))]
 
 
 class Phases:
@@ -186,10 +188,9 @@
 
     phase("enter")
     barrier = pltpu.get_barrier_semaphore()
-    near = [(wrap(y + dy, YN), wrap(x + dx, XN), z, c) for dy, dx in PLANE]
-    near += [(wrap(y + dy, YN), wrap(x + dx, XN), z, oc) for dy, dx in PLANE]
+    near = [(y, x, wrap(z + d, ZN), c) for d in ALONG_Z]
+    near += [(wrap(y + dy, YN), wrap(x + dx, XN), z, core) for dy, dx in PLANE for core in (c, oc)]
     near += [partner]
-    near += [(y, x, wrap(z + d, ZN), c) for d in ALONG_Z]
     for device in near:
         pl.semaphore_signal(barrier, inc=1, device_id=device, device_id_type=MESH_ID)
 
@@ -213,11 +214,8 @@
     load(qm_in, mas.at[0])
     load(km_in, mas.at[1])
     phase("loads")
-    for copy in loads:
+    for copy in loads[:3]:
         copy.wait()
-    masters[f, :, 0:HD] = mas[0].astype(BF)
-    masters[f, :, HD : 2 * HD] = mas[1].astype(BF)
-
     sends = Sends(send_sem, recv_sem)
     phase("barrier")
     pl.semaphore_wait(barrier, len(near))
@@ -247,6 +245,8 @@
         zz = wrap(z + d, ZN)
         rows = xs.at[pl.ds(pl.multiple_of(zz * SUB, SUB), SUB)]
         sends.start(sent_x, got_x, rows, xslot(z), (y, x, zz, c))
+    for copy in loads[3:]:
+        copy.wait()
 
     def swap(src, dst):
         received = sends.received_group()
@@ -256,6 +256,8 @@
     n_cot = swap(cots.at[oc], cot_other)
     n_mom = swap(mom.at[oc], mom_other)
     xg[:, pl.ds(pl.multiple_of(z * HD, HD), HD)] = xs[pl.ds(pl.multiple_of(z * SUB, SUB), SUB), :]
+    masters[f, :, 0:HD] = mas[0].astype(BF)
+    masters[f, :, HD : 2 * HD] = mas[1].astype(BF)
     phase("basis_1")
     next(gather_basis)
 
@@ -276,7 +278,6 @@
     for _ in gather_basis:
         pass
     phase("wait_x")
-    next(gather_masters)
     sends.landed(got_x, several, partner)
 
     phase("xb")
@@ -294,42 +295,38 @@
     xb[0] = (psend[c] + precv[...]).astype(BF)
 
     sent_z = sends.sent_group(xb.at[pl.ds(0, ZN - 1)])
-    nz = {o % ZN: sends.received_group() for o, _ in Z_RELAY}
+    nz = {(o % ZN, k): sends.received_group() for o, _ in Z_RELAY for k in range(CUTS)}
     rest_z = sends.received_group()
 
-    def z_send(o, d):
+    def z_send(o, d, k):
+        rows = pl.ds(k * CUT, CUT)
         sends.start(
             sent_z,
-            nz.get((o + d) % ZN, rest_z),
-            xb.at[o % ZN],
-            xb.at[(o + d) % ZN],
+            nz.get(((o + d) % ZN, k), rest_z),
+            xb.at[o % ZN, rows],
+            xb.at[(o + d) % ZN, rows],
             (y, x, wrap(z + d, ZN), c),
         )
 
-    def z_landed(o):
-        sends.landed(nz[o % ZN], xb.at[o % ZN], partner)
-
     phase("z_send")
     for d in Z_FIRST:
-        z_send(0, d)
+        for k in range(CUTS):
+            z_send(0, d, k)
     n_basis = swap(basis.at[:, c], basis.at[:, c])
     next(gather_masters)
+    next(gather_masters)
     phase("z_relay1")
-    for o, hops in Z_RELAY[:2]:
-        z_landed(o)
-        for d in hops:
-            z_send(o, d)
-    phase("z_relay2")
-    for o, hops in Z_RELAY[2:]:
-        z_landed(o)
-        for d in hops:
-            z_send(o, d)
+    for k in range(CUTS):
+        for o, hops in Z_RELAY:
+            sends.landed(nz[o % ZN, k], xb.at[o % ZN, pl.ds(k * CUT, CUT)], partner)
+            for d in hops:
+                z_send(o, d, k)
     phase("masters")
     next(gather_masters)
     next(gather_masters)
     next(gather_masters)
     phase("z_rest")
-    sends.landed(rest_z, xb.at[pl.ds(0, ZN - 1 - len(nz))], partner)
+    sends.landed(rest_z, xb.at[pl.ds(0, ZN - 1 - len(Z_RELAY))], partner)
     sends.landed(n_basis, basis.at[:, oc], partner)
 
     phase("low")
@@ -385,7 +382,7 @@
     phase(None)
 
 
-N_SENT, N_RECEIVED = 11, 43
+N_SENT, N_RECEIVED = 11, 43 + 4 * (CUTS - 1)
 
 
 GROUP = 4

time: 62.9 us -> 61.7 us (0.981)
  Pallas kernels: 62.1 us -> 60.9 us
    pallas_call x1, Pallas kernels: 59 us -> 57.8 us  [body(): pl.pallas_call(exchange, name='exchange', out_shape=(jax.ShapeDtypeStruct...]
where the time goes in v5:
time: 61.7 us; the launch traced here: 61.5 us
  Pallas kernels  60.9 us (99%)
  between operations  0.65 us (1%)
    pallas_call x1, Pallas kernels, body(): pl.pallas_call(exchange, name='exchange', out_shape=(jax.ShapeDtypeStruct...  57.8 us
    pallas_call x1, Pallas kernels, body(): pl.pallas_call(finish, name='finish', out_shape=(matrix, matrix, whole, m...  3.08 us

profile of v5, /device:TPU:1, one launch (start us, length us, event | category | flops | bytes accessed | tf_op | source)
XLA Modules:
  0.0 61.5 jit_solution(16571128264999709498)
XLA Ops:
  0.6 57.8 %exchange.1 = (bf16[16,2,128,512]{3,2,1,0:T(8,128)(2,1)S(1)}, bf16[16,256,256]{2,1,0:T(8,128)(2,1)S(1)}, bf16[2,16,16,128]{3,2,1,0:T(8,128)(2,1)S(1)}, f32[2,2,16,128]{3,2,1,0:T(8,128)S(1)}, f32[2,256,128]{2,1,0:T(8,128)S(1)}) custom-call(bf16[1024,128]{1,0:T(8,128)(2,1)} %x_in.1, bf16[1024,128]{1,0:T(8,128)(2,1)} %qc_in.1, bf16[1024,128]{1,0:T(8,128)(2,1)} %kc_in.1, ...), custom_call_target="tpu_custom_call" | custom-call | tf_op jit(solution)/shard_map/exchange/pallas_call | solution.py:449
  58.5 3.1 %finish.1 = (f32[256,128]{1,0:T(8,128)}, f32[256,128]{1,0:T(8,128)}, bf16[4096,128]{1,0:T(8,128)(2,1)}, f32[16,128]{1,0:T(8,128)}, f32[16,128]{1,0:T(8,128)}, /*...) custom-call(bf16[16,2,128,512]{3,2,1,0:T(8,128)(2,1)S(1)} %get-tuple, ...), custom_call_target="tpu_custom_call" | custom-call | tf_op jit(solution)/shard_map/finish/pallas_call | solution.py:489

commit v6 on v5

--- a/solution.py
+++ b/solution.py
@@ -39,7 +39,10 @@
 )
 ALONG_Z = [8, 7, -7, 6, -6, 5, -5, 4, -4, 3, -3, 2, -2, 1, -1]
 Z_FIRST = [5, -5, 2, -2, 1, -1]
-Z_RELAY = [(5, (3, 2, 1, -1)), (-5, (-2, -1, 1)), (2, (1,)), (-2, (-1,))]
+Z_RELAY = [
+    [(5, (3, 2, 1, -1)), (-5, (-2, -1, 1)), (2, (1,)), (-2, (-1,))],
+    [(5, (2, 1, -1)), (-5, (-3, -2, -1, 1)), (2, (1,)), (-2, (-1,))],
+]
 
 
 class Phases:
@@ -295,7 +298,7 @@
     xb[0] = (psend[c] + precv[...]).astype(BF)
 
     sent_z = sends.sent_group(xb.at[pl.ds(0, ZN - 1)])
-    nz = {(o % ZN, k): sends.received_group() for o, _ in Z_RELAY for k in range(CUTS)}
+    nz = {(o % ZN, k): sends.received_group() for k in range(CUTS) for o, _ in Z_RELAY[k]}
     rest_z = sends.received_group()
 
     def z_send(o, d, k):
@@ -317,7 +320,7 @@
     next(gather_masters)
     phase("z_relay1")
     for k in range(CUTS):
-        for o, hops in Z_RELAY:
+        for o, hops in Z_RELAY[k]:
             sends.landed(nz[o % ZN, k], xb.at[o % ZN, pl.ds(k * CUT, CUT)], partner)
             for d in hops:
                 z_send(o, d, k)
@@ -326,7 +329,7 @@
     next(gather_masters)
     next(gather_masters)
     phase("z_rest")
-    sends.landed(rest_z, xb.at[pl.ds(0, ZN - 1 - len(Z_RELAY))], partner)
+    sends.landed(rest_z, xb.at[pl.ds(0, ZN - 1 - len(Z_RELAY[0]))], partner)
     sends.landed(n_basis, basis.at[:, oc], partner)
 
     phase("low")
@@ -405,34 +408,35 @@
         copy.start()
         stores.append(copy)
 
-    phase("product")
-    ratio = [ratios[m].reshape(RANK, HD) for m in range(2)]
-    totals = [jnp.zeros((8, HD), F32) for _ in range(2)]
-    for g in range(GROUPS):
-        for k in range(g * GROUP, (g + 1) * GROUP):
-            for m in range(2):
-                rows = basis[k, :, :, m * RANK : (m + 1) * RANK].reshape(ROWS, RANK)
-                update = jnp.dot(rows, ratio[m], preferred_element_type=F32)
-                held[m, k] = update
-                totals[m] += jnp.sum((update * update).reshape(ROWS // 8, 8, HD), axis=0)
-    phase("scale")
-    for m, refs in enumerate(((q_first, q_second), (k_first, k_second))):
-        for i in range(2):
-            store(moments.at[m, i], refs[i])
-    scales = [1.0 / jnp.sqrt(jnp.sum(t) / (D * HD) + norm_floor) for t in totals]
-    for m, (step_ref, weight_ref) in enumerate(((q_step, q_weight), (k_step, k_weight))):
-        step = held[m, f] * scales[m]
+    outs = (
+        (q_step, q_weight, q_copy, q_first, q_second),
+        (k_step, k_weight, k_copy, k_first, k_second),
+    )
+    for m, (step_ref, weight_ref, copy_ref, first_ref, second_ref) in enumerate(outs):
+        store(moments.at[m, 0], first_ref)
+        store(moments.at[m, 1], second_ref)
+    for m, (step_ref, weight_ref, copy_ref, first_ref, second_ref) in enumerate(outs):
+        phase(f"product_{m}")
+        ratio = ratios[m].reshape(RANK, HD)
+        total = jnp.zeros((8, HD), F32)
+        for g in range(GROUPS):
+            blocks = slice(g * GROUP, (g + 1) * GROUP)
+            rows = basis[blocks, :, :, m * RANK : (m + 1) * RANK].reshape(GROUP * ROWS, RANK)
+            update = jnp.dot(rows, ratio, preferred_element_type=F32)
+            held[m, blocks] = update.reshape(GROUP, ROWS, HD)
+            total += jnp.sum((update * update).reshape(GROUP * ROWS // 8, 8, HD), axis=0)
+        phase(f"copies_{m}")
+        scale = 1.0 / jnp.sqrt(jnp.sum(total) / (D * HD) + norm_floor)
+        step = held[m, f] * scale
         steps[m] = step
         weights[m] = own[m] - step_rate * step
         store(steps.at[m], step_ref)
         store(weights.at[m], weight_ref)
-    phase("copies")
-    for g in range(GROUPS):
-        for m, copy_ref in enumerate((q_copy, k_copy)):
+        for g in range(GROUPS):
             for k in range(g * GROUP, (g + 1) * GROUP):
                 old = masters[k, :, m * HD : (m + 1) * HD].astype(F32)
                 copies[m, k * ROWS : (k + 1) * ROWS] = (
-                    old - step_rate * (held[m, k] * scales[m])
+                    old - step_rate * (held[m, k] * scale)
                 ).astype(BF)
             rows = pl.ds(g * GROUP * ROWS, GROUP * ROWS)
             store(copies.at[m, rows], copy_ref.at[rows])

time: 61.7 us -> 61.2 us (level)
  no operation moved by 1% of the time
where the time goes in v6:
time: 61.2 us; the launch traced here: 61 us
  Pallas kernels  60.4 us (99%)
  between operations  0.65 us (1%)
    pallas_call x1, Pallas kernels, body(): pl.pallas_call(exchange, name='exchange', out_shape=(jax.ShapeDtypeStruct...  57.4 us
    pallas_call x1, Pallas kernels, body(): pl.pallas_call(finish, name='finish', out_shape=(matrix, matrix, whole, m...  2.98 us

profile of v6, /device:TPU:1, one launch (start us, length us, event | category | flops | bytes accessed | tf_op | source)
XLA Modules:
  0.0 61.0 jit_solution(14108989319780238843)
XLA Ops:
  0.6 57.4 %exchange.1 = (bf16[16,2,128,512]{3,2,1,0:T(8,128)(2,1)S(1)}, bf16[16,256,256]{2,1,0:T(8,128)(2,1)S(1)}, bf16[2,16,16,128]{3,2,1,0:T(8,128)(2,1)S(1)}, f32[2,2,16,128]{3,2,1,0:T(8,128)S(1)}, f32[2,256,128]{2,1,0:T(8,128)S(1)}) custom-call(bf16[1024,128]{1,0:T(8,128)(2,1)} %x_in.1, bf16[1024,128]{1,0:T(8,128)(2,1)} %qc_in.1, bf16[1024,128]{1,0:T(8,128)(2,1)} %kc_in.1, ...), custom_call_target="tpu_custom_call" | custom-call | tf_op jit(solution)/shard_map/exchange/pallas_call | solution.py:453
  58.0 3.0 %finish.1 = (f32[256,128]{1,0:T(8,128)}, f32[256,128]{1,0:T(8,128)}, bf16[4096,128]{1,0:T(8,128)(2,1)}, f32[16,128]{1,0:T(8,128)}, f32[16,128]{1,0:T(8,128)}, /*...) custom-call(bf16[16,2,128,512]{3,2,1,0:T(8,128)(2,1)S(1)} %get-tuple, ...), custom_call_target="tpu_custom_call" | custom-call | tf_op jit(solution)/shard_map/finish/pallas_call | solution.py:493
